TPU v7x, 512 devices: a whole 4x8x8 slice. The times are simulated.
512 devices in a mesh: ep: 128 (over z, y, core), tp: 4 (over x).
Axes of the slice: x: 4, y: 8, z: 8, core: 2. Of those that a mesh axis runs over, the one named last changes fastest.
Arguments:
- tokens: bfloat16 [256, 2048], P('ep'), may hold values from -6 to 6
- state_c: float32 [256, 8, 128, 256], P('ep', 'tp'), may hold values from -0.8 to 0.8
- state_n: float32 [256, 8, 128], P('ep', 'tp'), may hold values from -0.8 to 0.8
- state_m: float32 [256, 8], P('ep', 'tp'), may hold values from -2 to 2
- mix_gain: float32 [2048], replicated, may hold values from 0.1 to 1.9
- w_query: bfloat16 [2048, 1024], P('ep', 'tp'), may hold values from -0.125 to 0.125
- w_key: bfloat16 [2048, 1024], P('ep', 'tp'), may hold values from -0.125 to 0.125
- w_value: bfloat16 [2048, 2048], P('ep', 'tp'), may hold values from -0.125 to 0.125
- w_input_gate: bfloat16 [2048, 8], replicated, may hold values from -0.125 to 0.125
- w_forget_gate: bfloat16 [2048, 8], replicated, may hold values from -0.125 to 0.125
- forget_bias: float32 [8], replicated, may hold values from -1 to 4
- w_output: bfloat16 [2048, 2048], P('tp', 'ep'), may hold values from -0.125 to 0.125
- moe_gain: float32 [2048], replicated, may hold values from 0.1 to 1.9
- w_group: bfloat16 [2048, 4], replicated, may hold values from -0.25 to 0.25
- expert_ids: int32 [256, 2], P('ep'), may hold values from 0 to 127, all different within a row; in each aligned block of 2 rows (0 to 1, 2 to 3, ...) at most 1 rows name the same one
- expert_weight: float32 [256, 2], P('ep'), may hold values from 0.1 to 1
- w_exp_gate: bfloat16 [128, 2048, 512], P('ep', None, 'tp'), may hold values from -0.125 to 0.125
- w_exp_up: bfloat16 [128, 2048, 512], P('ep', None, 'tp'), may hold values from -0.25 to 0.25
- w_exp_down: bfloat16 [128, 512, 2048], P('ep', 'tp'), may hold values from -1 to 1
- w_dense: bfloat16 [2048, 2048], P('ep', 'tp'), may hold values from -0.125 to 0.125
- w_dense_gate: bfloat16 [2048], replicated, may hold values from -0.125 to 0.125
Outputs:
- mixed: bfloat16 [256, 2048], P('ep', 'tp')
- new_c: float32 [256, 8, 128, 256], P('ep', 'tp')
- new_n: float32 [256, 8, 128], P('ep', 'tp')
- new_m: float32 [256, 8], P('ep', 'tp')
Inputs may be any that keep to these rules, and one draw needn't show every extreme that they name: `expert_ids`: each row names 2 different experts. In each aligned block of 2 rows (the rows of one index of ep) no expert is named by more than 1 row, a bound that some block reaches. Every expert is named by some row.
All inputs are finite; a program needn't handle non-finite values.
Results may differ from a plain program's by a relative error of at most 0.025.
Values may be sent and summed in bfloat16 or wider, within the bound.
A program may use at most 64 MiB of HBM per device.

v0:
```python
import jax
import jax.numpy as jnp
from jax import lax
from jax.sharding import PartitionSpec as P

CAP = 1


eps = 1e-06


def side_by_side(arrays, axis, dim, along):
    both = jnp.concatenate(arrays, axis=along)
    filled, at, finished = (lax.all_gather(both, axis, axis=dim, tiled=True), 0, [])
    for a in arrays:
        finished.append(lax.slice_in_dim(filled, at, at + a.shape[along], axis=along))
        at += a.shape[along]
    return tuple(finished)


def copy_for_each(shard, axis):
    copies = jnp.broadcast_to(shard, (lax.axis_size(axis), *shard.shape))
    return lax.all_to_all(copies, axis, split_axis=0, concat_axis=0, tiled=True)


def over_copies(shard, axis):
    everything = copy_for_each(shard, axis)
    return jnp.sum(everything.astype(jnp.float32), axis=0)


def in_blocks(shard, dim, count):
    before, after = (shard.shape[:dim], shard.shape[dim + 1 :])
    return jnp.moveaxis(shard.reshape(*before, count, -1, *after), dim, 0)


def sum_at_owner(shard, axis, dim):
    tiles = in_blocks(shard, dim, lax.axis_size(axis))
    arrived = lax.all_to_all(tiles, axis, split_axis=0, concat_axis=0, tiled=True)
    return arrived.astype(jnp.float32).sum(axis=0)


def rms_norm(values, gain):
    widened = values.astype(jnp.float32)
    inverse = lax.rsqrt(jnp.mean(widened * widened, axis=-1, keepdims=True) + eps)
    return (widened * inverse * gain).astype(jnp.bfloat16)


def rounded(values):
    return lax.optimization_barrier(values.astype(jnp.bfloat16)).astype(jnp.float32)


def memory_step(query_rows, key_rows, value_rows, in_gate, forget, state_c, state_n, state_m):
    seq_count, head_count = state_m.shape
    q_heads = query_rows.reshape(seq_count, head_count, -1)
    k_heads = key_rows.reshape(seq_count, head_count, -1) * q_heads.shape[-1] ** (-0.5)
    v_heads = value_rows.reshape(seq_count, head_count, -1)
    new_m = jnp.maximum(forget + state_m, in_gate)
    decay = jnp.exp(forget + state_m - new_m)
    inflow = jnp.exp(in_gate - new_m)
    new_c = (
        decay[..., None, None] * state_c
        + (inflow[..., None] * k_heads)[..., :, None] * v_heads[..., None, :]
    )
    new_n = decay[..., None] * state_n + inflow[..., None] * k_heads
    numer = jnp.einsum("shd,shde->she", q_heads, new_c, precision=lax.Precision.HIGHEST)
    denom = jnp.maximum(jnp.abs(jnp.sum(q_heads * new_n, axis=-1)), 1.0)
    heads = (numer / denom[..., None]).astype(jnp.bfloat16).reshape(seq_count, -1)
    return (heads, new_c, new_n, new_m)


def per_device(
    tokens,
    state_c,
    state_n,
    state_m,
    mix_gain,
    w_query,
    w_key,
    w_value,
    w_input_gate,
    w_forget_gate,
    forget_bias,
    w_output,
    moe_gain,
    w_group,
    expert_ids,
    expert_weight,
    w_exp_gate,
    w_exp_up,
    w_exp_down,
    w_dense,
    w_dense_gate,
):
    seq_count = tokens.shape[0]
    width = tokens.shape[1]
    tp_count = lax.axis_size("tp")
    ep_count = lax.axis_size("ep")
    tp_rank = lax.axis_index("tp")
    head_count = state_m.shape[1]
    share = width // tp_count
    normed = rms_norm(tokens, mix_gain)
    pieces = side_by_side((w_query, w_key, w_value), "ep", 0, 1)
    feature_cols = normed
    query_sum, key_sum, value_sum = tuple(
        (
            jnp.dot(feature_cols, weight_rows, preferred_element_type=jnp.float32)
            for weight_rows in pieces
        )
    )
    query_rows = rounded(query_sum)
    key_rows = rounded(key_sum)
    value_rows = rounded(value_sum)
    gate_all = jnp.dot(normed, w_input_gate, preferred_element_type=jnp.float32)
    forget_all = jax.nn.log_sigmoid(
        jnp.dot(normed, w_forget_gate, preferred_element_type=jnp.float32) + forget_bias
    )
    in_gate = lax.dynamic_slice_in_dim(gate_all, tp_rank * head_count, head_count, 1)
    forget = lax.dynamic_slice_in_dim(forget_all, tp_rank * head_count, head_count, 1)
    heads, new_c, new_n, new_m = memory_step(
        query_rows, key_rows, value_rows, in_gate, forget, state_c, state_n, state_m
    )
    partial_value = jnp.dot(
        heads,
        lax.all_gather(w_output, "ep", axis=1, tiled=True),
        preferred_element_type=jnp.float32,
    )
    mixer_sum = over_copies(partial_value.astype(jnp.bfloat16), "tp").astype(jnp.float32)
    residual = (tokens.astype(jnp.float32) + mixer_sum).astype(jnp.bfloat16)
    normed2 = rms_norm(residual, moe_gain)
    group_count = w_group.shape[1]
    group_prob = jax.nn.softmax(
        jnp.dot(normed2, w_group, preferred_element_type=jnp.float32), axis=-1
    )
    experts_here = w_exp_gate.shape[0]
    expert_count = experts_here * ep_count
    per_group = expert_count // group_count
    top_count = expert_ids.shape[1]
    member = (expert_ids // per_group)[..., None] == jnp.arange(group_count, dtype=jnp.int32)[
        None, None, :
    ]
    picked = jnp.sum(jnp.where(member, group_prob[:, None, :], 0.0), axis=-1)
    route = picked * expert_weight / jnp.sum(expert_weight, axis=1, keepdims=True)
    flat_ids = expert_ids.reshape(-1)
    assigned = flat_ids[:, None] == jnp.arange(expert_count, dtype=jnp.int32)[None, :]
    ranks = jnp.cumsum(assigned.astype(jnp.int32), axis=0) - 1
    own_rank = jnp.sum(jnp.where(assigned, ranks, 0), axis=1)
    slot_index = flat_ids * CAP + own_rank
    placing = (
        jnp.arange(expert_count * CAP, dtype=jnp.int32)[:, None] == slot_index[None, :]
    ).astype(jnp.bfloat16)
    repeated = jnp.repeat(normed2, top_count, axis=0)
    outgoing = jnp.dot(placing, repeated, preferred_element_type=jnp.float32).astype(jnp.bfloat16)
    outgoing = outgoing.reshape(expert_count, CAP, width)
    arrived = lax.all_to_all(outgoing, "ep", split_axis=0, concat_axis=0, tiled=True)
    slots = arrived.shape[1]
    grid_rows = arrived.reshape(ep_count, experts_here, slots, width)
    gate_act = jnp.einsum(
        "sxnd,xdf->sxnf", grid_rows, w_exp_gate, preferred_element_type=jnp.float32
    )
    up_act = jnp.einsum("sxnd,xdf->sxnf", grid_rows, w_exp_up, preferred_element_type=jnp.float32)
    hidden = (jax.nn.silu(gate_act) * up_act).astype(jnp.bfloat16)
    down_part = jnp.einsum("sxnf,xfd->sxnd", hidden, w_exp_down, preferred_element_type=jnp.float32)
    reduced = sum_at_owner(down_part.astype(jnp.bfloat16), "tp", 3).astype(jnp.bfloat16)
    returned = lax.all_to_all(
        reduced.reshape(expert_count, slots, share), "ep", split_axis=0, concat_axis=0, tiled=True
    )
    picked_rows = jnp.einsum(
        "ca,cd->ad",
        placing,
        returned.reshape(expert_count * CAP, share),
        preferred_element_type=jnp.float32,
    )
    moe = jnp.sum(route[..., None] * picked_rows.reshape(seq_count, top_count, share), axis=1)
    feature_cols = normed2
    dense_raw = jnp.dot(
        feature_cols,
        lax.all_gather(w_dense, "ep", axis=0, tiled=True),
        preferred_element_type=jnp.float32,
    )
    dense_gate = jax.nn.sigmoid(jnp.dot(normed2, w_dense_gate, preferred_element_type=jnp.float32))
    own_cols = lax.dynamic_slice_in_dim(residual, tp_rank * share, share, 1).astype(jnp.float32)
    mixed = (own_cols + moe + dense_gate[:, None] * dense_raw).astype(jnp.bfloat16)
    return (mixed, new_c, new_n, new_m)


def solution(mesh):
    placed = (
        P("ep", None),
        P("ep", "tp", None, None),
        P("ep", "tp", None),
        P("ep", "tp"),
        P(),
        P("ep", "tp"),
        P("ep", "tp"),
        P("ep", "tp"),
        P(),
        P(),
        P(),
        P("tp", "ep"),
        P(),
        P(),
        P("ep", None),
        P("ep", None),
        P("ep", None, "tp"),
        P("ep", None, "tp"),
        P("ep", "tp", None),
        P("ep", "tp"),
        P(),
    )
    return jax.shard_map(
        per_device,
        mesh=mesh,
        in_specs=placed,
        out_specs=(P("ep", "tp"), P("ep", "tp", None, None), P("ep", "tp", None), P("ep", "tp")),
        check_vma=False,
    )
```

profile of v0, /device:TPU:1, one launch (start us, length us, event | category | flops | bytes accessed | tf_op | source)
XLA Modules:
  0.0 283.7 jit_solution(10336514559572382456)
XLA Ops:
  7.2 0.0 copy-start
  7.2 0.0 all-gather.4.cloned.1.call-start
  7.2 1.4 pad_maximum_fusion
  8.6 0.0 all-gather.4.cloned.1.call-update
  8.6 0.0 all-gather.6.cloned.1.call-start
  8.7 0.7 all-gather.6.cloned.1.call-update
  9.4 0.0 all-gather.8.cloned.1.call-start
  9.4 0.7 all-gather.8.cloned.1.call-update
  10.1 0.8 fusion.41
  11.0 0.8 fusion.43
  11.8 0.9 fusion.57
  12.7 0.9 fusion.49
  13.6 0.8 subtract_exponential_fusion.1
  14.3 0.1 exponential_multiply_fusion
  14.4 0.8 reshape.144
  15.2 0.1 fusion.47
  15.3 86.7 %all-gather.4.cloned.1.call-done = bf16[2048,1024]{1,0:T(8,128)(2,1)} async-done(((bf16[16,1024]{1,0:T(8,128)(2,1)}), bf16[2048,1024]{1,0:T(8,128)(2,1)}) %all-gather.4.cloned.1.call-update) | async-done | bytes 4194320 | tf_op jit(solution)/shard_map/all_gather | solution.py:14
  102.0 1.5 convolution_convert_fusion.4
  103.5 1.5 convolution_convert_fusion.3
  105.0 2.0 fusion.9
  107.0 0.0 copy-start.6
  107.1 0.7 multiply_reduce_fusion
  107.7 0.1 multiply_add_fusion
  107.9 0.3 fusion.58
  108.2 0.1 fusion.48
  108.3 76.8 %all-gather.6.cloned.1.call-done = bf16[512,2048]{0,1:T(8,128)(2,1)} async-done(((bf16[512,16]{0,1:T(8,128)(2,1)}), bf16[512,2048]{0,1:T(8,128)(2,1)}) %all-gather.6.cloned.1.call-update) | async-done | bytes 2097168 | tf_op jit(solution)/shard_map/all_gather | solution.py:124
  185.1 2.2 convolution_convert_fusion.2
  187.3 0.0 copy-start.11
  187.3 0.6 broadcast_in_dim.15
  188.0 4.0 %all-to-all-start = ((bf16[4,2,2048]{2,1,0:T(2,128)(2,1)}), bf16[4,2,2048]{2,1,0:T(2,128)(2,1)S(1)}, u32[]{:S(2)}, u32[]{:S(2)}) async-start(bf16[4,2,2048]{2,1,0:T(2,128)(2,1)} %broadcast_in_dim.15), calls=%async_computation | async-start | bytes 65536 | tf_op jit(solution)/shard_map/all_to_all | solution.py:23
  191.9 0.2 select_reduce_fusion
  192.1 4.1 %all-to-all-done = bf16[4,2,2048]{2,1,0:T(2,128)(2,1)S(1)} async-done(((bf16[4,2,2048]{2,1,0:T(2,128)(2,1)}), bf16[4,2,2048]{2,1,0:T(2,128)(2,1)S(1)}, u32[]{:S(2)}, u32[]{:S(2)}) %all-to-all-start) | async-done | bytes 32800 | tf_op jit(solution)/shard_map/all_to_all | solution.py:23
  196.2 0.1 convert_reduce_fusion
  196.3 0.1 fusion.38
  196.5 0.1 fusion.40
  196.6 0.3 fusion
  196.8 0.5 broadcast.107
  197.4 1.0 reduce.2
  198.4 1.2 reshape.167
  199.5 11.0 %all-to-all-start.1 = ((bf16[128,2,1024]{2,1,0:T(2,128)(2,1)}), bf16[128,2,1024]{2,1,0:T(2,128)(2,1)S(1)}, u32[]{:S(2)}, u32[]{:S(2)}) async-start(bf16[128,2,1024]{2,1,0:T(2,128)(2,1)} %reshape.167), calls=%async_computation.1 | async-start | bytes 1048576 | tf_op jit(solution)/shard_map/all_to_all | solution.py:154
  210.5 0.1 iota_compare_fusion.3
  210.7 0.1 reduce_sum.99
  210.8 0.2 fusion.56
  211.0 20.3 %all-to-all-done.1 = bf16[128,2,1024]{2,1,0:T(2,128)(2,1)S(1)} async-done(((bf16[128,2,1024]{2,1,0:T(2,128)(2,1)}), bf16[128,2,1024]{2,1,0:T(2,128)(2,1)S(1)}, u32[]{:S(2)}, u32[]{:S(2)}) %all-to-all-start.1) | async-done | bytes 524320 | tf_op jit(solution)/shard_map/all_to_all | solution.py:154
  231.3 0.4 reshape.168
  231.7 0.4 convolution_bitcast_fusion.1
  232.2 0.7 convolution_convert_fusion
  232.9 0.8 copy.67
  233.7 3.5 %all-to-all-start.2 = ((bf16[4,128,1,1,512]{4,1,3,2,0:T(8,128)(2,1)}), bf16[4,128,1,1,512]{4,1,3,2,0:T(8,128)(2,1)S(1)}, u32[]{:S(2)}, u32[]{:S(2)}) async-start(bf16[4,128,1,1,512]{4,1,3,2,0:T(8,128)(2,1)} %bitcast.95), calls=%async_computation.2 | async-start | bytes 1048576 | tf_op jit(solution)/shard_map/all_to_all | solution.py:38
  237.2 0.2 fusion.51
  237.4 0.1 fusion.50
  237.5 0.2 fusion.46
  237.6 9.3 %all-to-all-done.2 = bf16[4,128,1,1,512]{4,1,3,2,0:T(8,128)(2,1)S(1)} async-done(((bf16[4,128,1,1,512]{4,1,3,2,0:T(8,128)(2,1)}), bf16[4,128,1,1,512]{4,1,3,2,0:T(8,128)(2,1)S(1)}, u32[]{:S(2)}, u32[]{:S(2)}) %all-to-all-start.2) | async-done | bytes 524320 | tf_op jit(solution)/shard_map/all_to_all | solution.py:38
  247.0 0.1 reduce_sum.101
  247.0 0.7 reduce.3
  247.7 0.7 reshape.169
  248.4 5.8 %all-to-all-start.3 = ((bf16[128,2,256]{2,1,0:T(2,128)(2,1)}), bf16[128,2,256]{2,1,0:T(2,128)(2,1)S(1)}, u32[]{:S(2)}, u32[]{:S(2)}) async-start(bf16[128,2,256]{2,1,0:T(2,128)(2,1)} %reshape.169), calls=%async_computation.3 | async-start | bytes 262144 | tf_op jit(solution)/shard_map/all_to_all | solution.py:164
  254.2 0.1 multiply_divide_fusion
  254.3 0.1 fusion.16
  254.4 13.1 %all-to-all-done.3 = bf16[128,2,256]{2,1,0:T(2,128)(2,1)S(1)} async-done(((bf16[128,2,256]{2,1,0:T(2,128)(2,1)}), bf16[128,2,256]{2,1,0:T(2,128)(2,1)S(1)}, u32[]{:S(2)}, u32[]{:S(2)}) %all-to-all-start.3) | async-done | bytes 131104 | tf_op jit(solution)/shard_map/all_to_all | solution.py:164
  267.5 0.1 reshape.170
  267.6 0.2 fusion.6
  267.8 6.8 %all-gather.8.cloned.1.call-done = bf16[2048,512]{1,0:T(8,128)(2,1)} async-done(((bf16[16,512]{1,0:T(8,128)(2,1)}), bf16[2048,512]{1,0:T(8,128)(2,1)}) %all-gather.8.cloned.1.call-update) | async-done | bytes 2097168 | tf_op jit(solution)/shard_map/all_gather | solution.py:177
  274.6 2.6 fusion.8
  (38 shorter events, 0.3 us)
Async XLA Ops:
  7.2 225.0 %copy-start = (bf16[1,128,2048]{2,1,0:T(8,128)(2,1)S(1)}, bf16[1,128,2048]{2,1,0:T(8,128)(2,1)}, u32[]{:S(2)}) copy-start(bf16[1,128,2048]{2,1,0:T(8,128)(2,1)} %param.39) | copy-start | bytes 1572868
  7.2 94.9 %all-gather.4.cloned.1.call-start = ((), (), s32[]{:S(2)}) async-start(), calls=%async_computation.4 | async-start | bytes 4227072 | tf_op jit(solution)/shard_map/all_gather | solution.py:14
  8.6 176.4 %all-gather.6.cloned.1.call-start = ((), (), s32[]{:S(2)}) async-start(), calls=%async_computation.5 | async-start | bytes 2113536 | tf_op jit(solution)/shard_map/all_gather | solution.py:124
  9.4 265.2 %all-gather.8.cloned.1.call-start = ((), (), s32[]{:S(2)}) async-start(), calls=%async_computation.6 | async-start | bytes 2113536 | tf_op jit(solution)/shard_map/all_gather | solution.py:177
  14.3 92.7 %copy-start.9 = (f32[2,2]{1,0:T(2,128)}, f32[2,2]{1,0:T(2,128)S(1)}, u32[]{:S(2)}) copy-start(f32[2,2]{1,0:T(2,128)S(1)} %get-tuple-element.10) | copy-start | bytes 52
  15.3 91.8 %copy-start.10 = (f32[2,2,128]{2,1,0:T(2,128)S(1)}, f32[2,2,128]{2,1,0:T(2,128)}, u32[]{:S(2)}) copy-start(f32[2,2,128]{2,1,0:T(2,128)} %param.23) | copy-start | bytes 6148
  15.3 92.4 %copy-start.2 = (f32[2,2,128,256]{3,2,1,0:T(8,128)S(1)}, f32[2,2,128,256]{3,2,1,0:T(8,128)}, u32[]{:S(2)}) copy-start(f32[2,2,128,256]{3,2,1,0:T(8,128)} %param.22) | copy-start | bytes 1572868
  107.0 89.3 %copy-start.5 = (bf16[2,2048]{1,0:T(2,128)(2,1)S(1)}, bf16[2,2048]{1,0:T(2,128)(2,1)}, u32[]{:S(2)}) copy-start(bf16[2,2048]{1,0:T(2,128)(2,1)} %param.21) | copy-start | bytes 24580
  107.0 89.4 %copy-start.6 = (f32[2048]{0:T(1024)S(1)}, f32[2048]{0:T(1024)}, u32[]{:S(2)}) copy-start(f32[2048]{0:T(1024)} %param.33) | copy-start | bytes 24580
  107.9 90.5 %copy-start.1 = (f32[2,2,128,256]{3,2,1,0:T(8,128)}, f32[2,2,128,256]{3,2,1,0:T(8,128)S(1)}, u32[]{:S(2)}) copy-start(f32[2,2,128,256]{3,2,1,0:T(8,128)S(1)} %multiply_add_fusion) | copy-start | bytes 1572868
  187.3 23.3 %copy-start.7 = (bf16[2048]{0:T(1024)(128)(2,1)S(1)}, bf16[2048]{0:T(1024)(128)(2,1)}, u32[]{:S(2)}) copy-start(bf16[2048]{0:T(1024)(128)(2,1)} %param.41) | copy-start | bytes 12292
  187.3 23.3 %copy-start.8 = (f32[2,2]{1,0:T(2,128)S(1)}, f32[2,2]{1,0:T(2,128)}, u32[]{:S(2)}) copy-start(f32[2,2]{1,0:T(2,128)} %param.36) | copy-start | bytes 52
  187.3 23.5 %copy-start.11 = (s32[2,2]{1,0:T(2,128)S(1)}, s32[2,2]{1,0:T(2,128)}, u32[]{:S(2)}) copy-start(s32[2,2]{1,0:T(2,128)} %param.35) | copy-start | bytes 52
  187.3 23.5 %copy-start.12 = (bf16[2048,4]{0,1:T(4,128)(2,1)S(1)}, bf16[2048,4]{0,1:T(4,128)(2,1)}, u32[]{:S(2)}) copy-start(bf16[2048,4]{0,1:T(4,128)(2,1)} %param.34) | copy-start | bytes 49156
  188.0 8.3 %all-to-all-start = ((bf16[4,2,2048]{2,1,0:T(2,128)(2,1)}), bf16[4,2,2048]{2,1,0:T(2,128)(2,1)S(1)}, u32[]{:S(2)}, u32[]{:S(2)}) async-start(bf16[4,2,2048]{2,1,0:T(2,128)(2,1)} %broadcast_in_dim.15), calls=%async_computation | async-start | bytes 65536 | tf_op jit(solution)/shard_map/all_to_all | solution.py:23
  198.4 33.4 %copy-start.3 = (bf16[1,2048,128]{2,1,0:T(8,128)(2,1)S(1)}, bf16[1,2048,128]{2,1,0:T(8,128)(2,1)}, u32[]{:S(2)}) copy-start(bf16[1,2048,128]{2,1,0:T(8,128)(2,1)} %param.37) | copy-start | bytes 1572868
  199.5 32.6 %copy-start.4 = (bf16[1,2048,128]{2,1,0:T(8,128)(2,1)S(1)}, bf16[1,2048,128]{2,1,0:T(8,128)(2,1)}, u32[]{:S(2)}) copy-start(bf16[1,2048,128]{2,1,0:T(8,128)(2,1)} %param.38) | copy-start | bytes 1572868
  199.5 31.7 %all-to-all-start.1 = ((bf16[128,2,1024]{2,1,0:T(2,128)(2,1)}), bf16[128,2,1024]{2,1,0:T(2,128)(2,1)S(1)}, u32[]{:S(2)}, u32[]{:S(2)}) async-start(bf16[128,2,1024]{2,1,0:T(2,128)(2,1)} %reshape.167), calls=%async_computation.1 | async-start | bytes 1048576 | tf_op jit(solution)/shard_map/all_to_all | solution.py:154
  233.7 13.2 %all-to-all-start.2 = ((bf16[4,128,1,1,512]{4,1,3,2,0:T(8,128)(2,1)}), bf16[4,128,1,1,512]{4,1,3,2,0:T(8,128)(2,1)S(1)}, u32[]{:S(2)}, u32[]{:S(2)}) async-start(bf16[4,128,1,1,512]{4,1,3,2,0:T(8,128)(2,1)} %bitcast.95), calls=%async_computation.2 | async-start | bytes 1048576 | tf_op jit(solution)/shard_map/all_to_all | solution.py:38
  248.4 19.1 %all-to-all-start.3 = ((bf16[128,2,256]{2,1,0:T(2,128)(2,1)}), bf16[128,2,256]{2,1,0:T(2,128)(2,1)S(1)}, u32[]{:S(2)}, u32[]{:S(2)}) async-start(bf16[128,2,256]{2,1,0:T(2,128)(2,1)} %reshape.169), calls=%async_computation.3 | async-start | bytes 262144 | tf_op jit(solution)/shard_map/all_to_all | solution.py:164
Sparse Core Ops, SparseCore 0:
  11.7 90.3 all-gather.3
  105.2 79.8 all-gather.5
  188.2 86.3 all-gather.7
where the time goes:
time: 285 us; the launch traced here: 284 us
  waiting for transfers between devices  219 us (77%)
  starting transfers between devices  24.3 us (9%)
  between operations  14 us (5%)
  matrix products  13.7 us (5%)
  other arithmetic  7.77 us (3%)
  local copies, waits for them, and re-layouts  5.32 us (2%)
    all_gather x1, waiting for transfers between devices, side_by_side(): lax.all_gather(both, axis, axis=dim, tiled=True)  86.7 us
    all_gather x1, waiting for transfers between devices, per_device(): lax.all_gather(w_output, 'ep', axis=1, tiled=True)  76.8 us
    all_to_all x1, waiting for transfers between devices, per_device(): lax.all_to_all(outgoing, 'ep', split_axis=0, concat_axis=0, tiled=True)  20.3 us
    all_to_all x1, waiting for transfers between devices, per_device(): lax.all_to_all(reduced.reshape(expert_count, slots, share), 'ep', split_a...  13.1 us
    all_to_all x1, starting transfers between devices, per_device(): lax.all_to_all(outgoing, 'ep', split_axis=0, concat_axis=0, tiled=True)  11 us
    all_to_all x1, waiting for transfers between devices, sum_at_owner(): lax.all_to_all(tiles, axis, split_axis=0, concat_axis=0, tiled=True)  9.33 us
    all_gather x1, waiting for transfers between devices, per_device(): lax.all_gather(w_dense, 'ep', axis=0, tiled=True)  6.85 us
    all_to_all x1, starting transfers between devices, per_device(): lax.all_to_all(reduced.reshape(expert_count, slots, share), 'ep', split_a...  5.81 us
  transfers between devices with their start and end apart: 7, of which 7 were waited for; matrix products, arithmetic and copies ran while one was open for 8% of the time, Pallas kernels for 0%

commit v1 on v0

v1 whole, which is shorter than its diff:
```python
import jax
import jax.numpy as jnp
from jax import lax
from jax.experimental import pallas as pl
from jax.experimental.pallas import tpu as pltpu
from jax.sharding import PartitionSpec as P

NY = 8
NC = 2
eps = 1e-06
BF = jnp.bfloat16
F32 = jnp.float32
MESH = pl.DeviceIdType.MESH
NN = (((1,), (0,)), ((), ()))
NT = (((1,), (1,)), ((), ()))
TN = (((0,), (0,)), ((), ()))


def mm(a, b, dims=NN, precision=None):
    return lax.dot_general(a, b, dims, precision=precision, preferred_element_type=F32)


def iota(shape, dim):
    return lax.broadcasted_iota(jnp.int32, shape, dim)


def ones_where(mask):
    return jnp.where(mask, 1.0, 0.0).astype(BF)


def each(count, body):
    def step(d, carry):
        body(d)
        return carry

    lax.fori_loop(1, count, step, 0)


def wait_for(ref, sem):
    pltpu.make_async_copy(ref, ref, sem).wait()


def layer_kernel(
    n_ep,
    n_tp,
    tokens,
    state_c,
    state_n,
    state_m,
    mix_gain,
    w_query,
    w_key,
    w_value,
    w_in,
    w_forget,
    forget_bias,
    w_out,
    moe_gain,
    w_group,
    expert_ids,
    expert_weight,
    w_gate,
    w_up,
    w_down,
    w_dense,
    w_dense_gate,
    mixed,
    new_c,
    new_n,
    new_m,
    nrm,
    tn,
    tr,
    meta_own,
    meta,
    wqkv,
    wot,
    wd,
    pb,
    rb,
    c_in,
    c_out,
    hb,
    hg,
    op,
    og,
    res,
    ag,
    n2,
    n2z,
    wg,
    wu,
    wdn,
    dp,
    xg,
    eo,
    zg,
    ys,
    yg,
    loads,
    sent,
    got,
    got_z,
    count,
):
    nz = n_ep // (NY * NC)
    rows = w_query.shape[0]
    width = tokens.shape[1]
    block = NY * NC * rows
    nzc, nyc = nz * NC, NY * NC
    half = nz * NC
    seqs = 2 * n_ep
    share = width // n_tp
    qk = w_query.shape[1]
    lanes = wd.shape[1]
    group_count = w_group.shape[0]

    ep = lax.axis_index("ep")
    x = lax.axis_index("tp")
    z = ep // nyc
    y = (ep // NC) % NY
    c = ep % NC
    zc = z * NC + c
    yc = y * NC + c

    def device(z_, y_, c_, x_):
        return {"ep": (z_ * NY + y_) * NC + c_, "tp": x_}

    def send(src, dst, s, r, to):
        pltpu.make_async_remote_copy(
            src_ref=src, dst_ref=dst, send_sem=s, recv_sem=r, device_id=to, device_id_type=MESH
        ).start()

    def y_peer(d):
        return device(z, (y + d) % NY, c, x)

    def zc_peer(d):
        other = (zc + d) % nzc
        return other // NC, other, device(other // NC, y, other % NC, x)

    def xc_peer(d):
        other = (x * NC + c + d) % (n_tp * NC)
        return device(z, y, other % NC, other // NC)

    load_c = pltpu.make_async_copy(state_c, c_in, loads.at[0])
    load_g = pltpu.make_async_copy(w_gate.at[0], wg, loads.at[1])
    load_u = pltpu.make_async_copy(w_up.at[0], wu, loads.at[2])
    load_d = pltpu.make_async_copy(w_down.at[0], wdn, loads.at[3])
    for copy in (load_c, load_g, load_u, load_d):
        copy.start()

    wqkv[...] = jnp.zeros_like(wqkv)
    wot[...] = jnp.zeros_like(wot)
    wd[...] = jnp.zeros_like(wd)

    barrier = pltpu.get_barrier_semaphore()

    def greet(to):
        pl.semaphore_signal(barrier, inc=1, device_id=to, device_id_type=MESH)

    each(NY, lambda d: greet(y_peer(d)))
    each(nzc, lambda d: greet(zc_peer(d)[2]))
    each(n_tp * NC, lambda d: greet(xc_peer(d)))

    wide = tokens[...].astype(F32)
    inverse = lax.rsqrt(jnp.mean(wide * wide, axis=-1, keepdims=True) + eps)
    nrm[...] = jnp.zeros_like(nrm)
    nrm[0:2, :] = (wide * inverse * mix_gain[...]).astype(BF)
    lane = iota((2, 128), 1)
    idf = expert_ids[...].astype(F32)
    ewt = expert_weight[...]
    ew_hi = ewt.astype(BF).astype(F32)
    ew_lo = ewt - ew_hi
    packed = jnp.zeros((2, 128), F32)
    for k, part in enumerate((idf, ew_hi, ew_lo)):
        for j in range(2):
            packed = jnp.where(lane == 2 * k + j, part[:, j : j + 1], packed)
    meta_own[...] = jnp.zeros_like(meta_own)
    meta_own[0:2, :] = packed.astype(BF)

    own = pl.ds(pl.multiple_of(yc * rows, rows), rows)
    wqkv[own, 0:qk] = w_query[...]
    wqkv[own, qk : 2 * qk] = w_key[...]
    wqkv[own, 2 * qk :] = w_value[...]
    wot[own, :] = w_out[...]
    start = yc * rows
    dense_block = start // lanes
    dense_rows = pl.ds(pl.multiple_of(start % lanes, rows), rows)
    wd[z, dense_rows, :] = w_dense[...]

    pl.semaphore_wait(barrier, (NY - 1) + (nzc - 1) + (n_tp * NC - 1))

    def send_projection(d):
        to = y_peer(d)
        send(w_query, wqkv.at[own, pl.ds(0, qk)], sent.at[0], got.at[0], to)
        send(w_key, wqkv.at[own, pl.ds(qk, qk)], sent.at[0], got.at[0], to)
        send(w_value, wqkv.at[own, pl.ds(2 * qk, 2 * qk)], sent.at[0], got.at[0], to)

    def pair(index):
        return pl.ds(pl.multiple_of(2 * index, 2), 2)

    def cols(index):
        return pl.ds(pl.multiple_of(index * block, block), block)

    def send_rows(d):
        z_, _, to = zc_peer(d)
        send(nrm.at[0:2, cols(z_)], tn.at[pair(zc), :], sent.at[1], got.at[1], to)

    def send_raw(d):
        z_, _, to = zc_peer(d)
        send(tokens.at[:, cols(z_)], tr.at[pair(zc), :], sent.at[2], got.at[2], to)
        send(meta_own.at[0:2, :], meta.at[y, pair(zc), :], sent.at[3], got.at[3], to)

    each(nzc, send_rows)
    each(NY, send_projection)
    each(NY, lambda d: send(w_out, wot.at[own, :], sent.at[4], got.at[4], y_peer(d)))
    each(nzc, send_raw)
    each(
        nz,
        lambda d: send(
            w_dense,
            wd.at[z, dense_rows, :],
            sent.at[5],
            got.at[5],
            device((z + d) % nz, y, c, x),
        ),
    )
    keep_n = pltpu.make_async_copy(nrm.at[0:2, cols(z)], tn.at[pair(zc), :], loads.at[4])
    keep_r = pltpu.make_async_copy(tokens.at[:, cols(z)], tr.at[pair(zc), :], loads.at[5])
    keep_m = pltpu.make_async_copy(meta_own.at[0:2, :], meta.at[y, pair(zc), :], loads.at[6])
    for copy in (keep_n, keep_r, keep_m):
        copy.start()

    head_count = state_m.shape[1]
    gate_all = mm(nrm[...], w_in[...], NT)[0:2]
    raw = mm(nrm[...], w_forget[...], NT)[0:2] + forget_bias[...]
    forget_all = jnp.minimum(raw, 0.0) - jnp.log1p(jnp.exp(-jnp.abs(raw)))
    head_lane = iota(gate_all.shape, 1)

    def of_head(values, h):
        mine = head_lane == x * head_count + h
        return jnp.sum(jnp.where(mine, values, 0.0), axis=1, keepdims=True)

    decays, inflows, ms = [], [], []
    for h in range(head_count):
        gate_h, forget_h = of_head(gate_all, h), of_head(forget_all, h)
        kept = forget_h + state_m[:, h : h + 1]
        m_h = jnp.maximum(kept, gate_h)
        decays.append(jnp.exp(kept - m_h))
        inflows.append(jnp.exp(gate_h - m_h))
        ms.append(m_h)
    m_lane = iota(state_m.shape, 1)
    new_m_value = jnp.zeros(state_m.shape, F32)
    for h in range(head_count):
        new_m_value = jnp.where(m_lane == h, ms[h], new_m_value)
    new_m[...] = new_m_value

    keep_m.wait()
    wait_for(count.at[0 : nzc - 1, :, 0:128], got.at[3])
    each(NY, lambda d: send(meta.at[y], meta.at[y], sent.at[6], got.at[6], y_peer(d)))

    keep_n.wait()
    wait_for(count.at[0 : nzc - 1, :, 0:block], got.at[1])
    wait_for(wqkv.at[0 : (NY - 1) * rows, :], got.at[0])
    pb[...] = mm(tn[...], wqkv[...]).astype(BF)
    keep_p = pltpu.make_async_copy(pb.at[pair(zc), :], rb.at[pair(zc), :], loads.at[4])
    keep_p.start()

    def send_partial(d):
        _, other, to = zc_peer(d)
        send(pb.at[pair(other), :], rb.at[pair(zc), :], sent.at[7], got.at[7], to)

    each(nzc, send_partial)
    load_c.wait()
    keep_p.wait()
    wait_for(count.at[0 : nzc - 1, :, 0:4 * qk], got.at[7])

    def pair_sum(count):
        r, col = iota((16, 2 * count), 0), iota((16, 2 * count), 1)
        return ones_where((col & 1) == r)

    rows_sum = mm(pair_sum(nzc), rb[...]).astype(BF)

    row = iota((16, 1), 0)
    dqk, dv = state_c.shape[2], state_c.shape[3]
    for h in range(head_count):
        q = rows_sum[:, h * dqk : (h + 1) * dqk]
        k = rows_sum[:, qk + h * dqk : qk + (h + 1) * dqk]
        v = rows_sum[:, 2 * qk + h * dv : 2 * qk + (h + 1) * dv]
        qf, kf = q.astype(F32), k.astype(F32)
        heads = jnp.zeros((16, dv), F32)
        for t in range(2):
            decay = decays[h][t : t + 1, :]
            inflow = inflows[h][t : t + 1, :] * dqk ** (-0.5)
            outer = mm(jnp.where(row == t, kf, 0.0).astype(BF), v, TN)
            c_new = decay * c_in[t, h] + inflow * outer
            c_out[t, h] = c_new
            n_new = decay * state_n[t, h : h + 1, :] + inflow * kf[t : t + 1, :]
            new_n[t, h : h + 1, :] = n_new
            numer = mm(qf, c_new, precision=lax.Precision.HIGHEST)
            denom = jnp.sum(qf[t : t + 1, :] * n_new, axis=-1, keepdims=True)
            denom = jnp.maximum(jnp.abs(denom), 1.0)
            heads = jnp.where(row == t, numer / denom, heads)
        hb[:, h * dv : (h + 1) * dv] = heads.astype(BF)
    store_c = pltpu.make_async_copy(c_out, new_c, loads.at[0])
    store_c.start()

    keep_h = pltpu.make_async_copy(hb.at[0:2, :], hg.at[pair(zc), :], loads.at[4])
    keep_h.start()
    each(
        nzc,
        lambda d: send(
            hb.at[0:2, :], hg.at[pair(zc), :], sent.at[8], got.at[8], zc_peer(d)[2]
        ),
    )
    wait_for(wot.at[0 : (NY - 1) * rows, :], got.at[4])
    keep_r.wait()
    wait_for(count.at[0 : nzc - 1, :, 0:block], got.at[2])
    keep_h.wait()
    wait_for(count.at[0 : nzc - 1, :, 0:2 * qk], got.at[8])
    part = mm(hg[...], wot[...], NT).astype(BF)
    op[...] = part
    xc = x * NC + c
    og[xc] = part
    each(n_tp * NC, lambda d: send(op, og.at[xc], sent.at[9], got.at[9], xc_peer(d)))
    wait_for(og.at[0 : n_tp * NC - 1], got.at[9])
    parts = jnp.zeros((2 * nzc, block), F32)
    for k in range(n_tp * NC):
        parts = parts + og[k].astype(F32)
    res[...] = (tr[...].astype(F32) + parts).astype(BF)

    sa = z + c * (y - z)
    sb = y + c * (z - y)

    def at(a, b):
        return device(a + c * (b - a), b + c * (a - b), c, x)

    ag[c, sa, sb] = res[pl.ds(pl.multiple_of(c * half, half), half), :]
    mine = ag.at[c, sa, sb]
    each(NY, lambda d: send(mine, mine, sent.at[10], got.at[10], at(sa, (sb + d) % NY)))
    wait_for(ag.at[0, 0, 0 : NY - 1], got.at[10])
    line = ag.at[c, sa]
    partner = device(z, y, 1 - c, x)
    each(nz, lambda d: send(line, line, sent.at[11], got_z.at[d], at((sa + d) % nz, sb)))
    send(line, line, sent.at[12], got.at[11], partner)

    def pass_on(d):
        arrived = ag.at[c, (sa + nz - d) % nz]
        wait_for(arrived, got_z.at[d])
        send(arrived, arrived, sent.at[12], got.at[11], partner)

    each(nz, pass_on)
    wait_for(meta.at[0 : NY - 1], got.at[6])
    for copy in (load_g, load_u, load_d):
        copy.wait()
    wait_for(ag.at[0], got.at[11])

    side = seqs // 2

    def rows_of(h, b):
        values = ag[0, b] if h == 0 else ag[1, :, b]
        return values.reshape(side, block)

    for h in range(2):
        squares = jnp.zeros((side, block), F32)
        for b in range(nz):
            piece = rows_of(h, b).astype(F32)
            squares = squares + piece * piece
        mean = jnp.sum(squares, axis=-1, keepdims=True) * (1.0 / width)
        inverse = lax.rsqrt(mean + eps)
        for b in range(nz):
            piece = rows_of(h, b).astype(F32)
            gain = moe_gain[:, b * block : (b + 1) * block]
            n2[h * side : (h + 1) * side, b * block : (b + 1) * block] = (
                piece * inverse * gain
            ).astype(BF)

    gate_act = mm(n2[...], wg[...])
    up_act = mm(n2[...], wu[...])
    hidden = gate_act * jax.nn.sigmoid(gate_act) * up_act
    meta_rows = jnp.concatenate(
        [meta[:, h * half : (h + 1) * half, :].reshape(side, 128) for h in range(2)], axis=0
    )
    mf = meta_rows.astype(F32)
    expert = ep.astype(F32)
    assigned = (mf[:, 0:1] == expert) | (mf[:, 1:2] == expert)
    hidden = jnp.where(assigned, hidden, 0.0).astype(BF)

    def token_of(shape):
        r = iota(shape, 1)
        h, y_, rest = r // side, (r // half) % NY, r % half
        z_ = h * (nz // 2) + rest // (2 * NC)
        return ((z_ * NY + y_) * NC) * 2 + rest % (2 * NC)

    slot_rows = iota((n_ep, seqs), 0)
    placing = ones_where(token_of((n_ep, seqs)) // 2 == slot_rows)
    slots = mm(placing, hidden).astype(BF)

    def down(x_):
        return mm(slots, wdn[:, pl.ds(pl.multiple_of(x_ * share, share), share)]).astype(BF)

    for d in range(1, n_tp):
        x_ = (x + d) % n_tp
        dp[d] = down(x_)
        send(dp.at[d], xg.at[x], sent.at[13], got.at[12], device(z, y, c, x_))
    xg[x] = down(x)

    local = ones_where(token_of((2 * nyc, seqs)) == z * 2 * nyc + iota((2 * nyc, seqs), 0))
    picks = mm(local, meta_rows)
    zrows = mm(local, n2[...]).astype(BF)
    n2z[...] = zrows
    wait_for(wd.at[0 : nz - 1, 0:rows, :], got.at[5])
    dense = jnp.zeros((2 * nyc, share), F32)
    for b in range(nz):
        at_lane = pl.multiple_of(b * block + dense_block * lanes, lanes)
        dense = dense + mm(n2z[:, pl.ds(at_lane, lanes)], wd[b])
    dense_gate = jnp.sum(
        zrows.astype(F32) * w_dense_gate[...].astype(F32), axis=-1, keepdims=True
    )
    dense = jax.nn.sigmoid(dense_gate) * dense
    logits = mm(zrows, w_group[...], NT)
    shifted = jnp.exp(logits - jnp.max(logits, axis=-1, keepdims=True))
    prob = shifted / jnp.sum(shifted, axis=-1, keepdims=True)
    per_group = n_ep // group_count
    first = (iota(prob.shape, 1) * per_group).astype(F32)
    weights = [picks[:, 2 + j : 3 + j] + picks[:, 4 + j : 5 + j] for j in range(2)]
    total = weights[0] + weights[1]
    at_slot = iota((2 * nyc, n_ep), 1)
    source = ((at_slot // nyc) * nyc + yc).astype(F32)
    same = at_slot % nyc == iota((2 * nyc, n_ep), 0) // 2
    mixing = jnp.zeros((2 * nyc, n_ep), F32)
    for j in range(2):
        ident = picks[:, j : j + 1]
        member = (ident >= first) & (ident < first + per_group)
        picked = jnp.sum(jnp.where(member, prob, 0.0), axis=-1, keepdims=True)
        route = picked * weights[j] / total
        mixing = mixing + jnp.where(same & (ident == source), route, 0.0)
    mix_hi = mixing.astype(BF)
    mix_lo = (mixing - mix_hi.astype(F32)).astype(BF)
    owned = ones_where(
        (token_of((16, seqs)) == 2 * ep + iota((16, seqs), 0)) & (iota((16, seqs), 0) < 2)
    )
    per_share = nz // n_tp
    residual = []
    for k in range(per_share):
        b = x * per_share + k
        residual.append(
            mm(owned[:, 0:side], ag[0, b].reshape(side, block))
            + mm(owned[:, side:], ag[1, :, b].reshape(side, block))
        )

    wait_for(xg.at[0 : n_tp - 1], got.at[12])
    total_out = xg[0].astype(F32)
    for k in range(1, n_tp):
        total_out = total_out + xg[k].astype(F32)
    eo[...] = total_out.astype(BF)

    def slots_of(z_):
        return eo.at[pl.ds(pl.multiple_of(z_ * nyc, nyc), nyc), :]

    each(
        nz,
        lambda d: send(
            slots_of((z + d) % nz), zg.at[z], sent.at[14], got.at[13], device((z + d) % nz, y, c, x)
        ),
    )
    zg[z] = eo[pl.ds(pl.multiple_of(z * nyc, nyc), nyc), :]
    wait_for(zg.at[0 : nz - 1], got.at[13])
    arrived = zg[...].reshape(n_ep, share)
    ys[...] = (mm(mix_hi, arrived) + mm(mix_lo, arrived) + dense).astype(BF)
    keep_y = pltpu.make_async_copy(ys.at[pair(yc), :], yg.at[pair(yc), :], loads.at[4])
    keep_y.start()

    def send_sums(d):
        other = (yc + d) % nyc
        to = device(z, other // NC, other % NC, x)
        send(ys.at[pair(other), :], yg.at[pair(yc), :], sent.at[15], got.at[14], to)

    each(nyc, send_sums)
    keep_y.wait()
    wait_for(count.at[0 : nyc - 1, :, 0:share], got.at[14])
    summed = mm(pair_sum(nyc), yg[...])
    for k in range(per_share):
        at_cols = slice(k * block, (k + 1) * block)
        mixed[:, at_cols] = (residual[k] + summed[:, at_cols])[0:2].astype(BF)

    store_c.wait()
    wait_for(wqkv.at[0 : (NY - 1) * rows, :], sent.at[0])
    wait_for(count.at[0 : nzc - 1, :, 0:block], sent.at[1])
    wait_for(count.at[0 : nzc - 1, :, 0:block], sent.at[2])
    wait_for(count.at[0 : nzc - 1, :, 0:128], sent.at[3])
    wait_for(wot.at[0 : (NY - 1) * rows, :], sent.at[4])
    wait_for(wd.at[0 : nz - 1, 0:rows, :], sent.at[5])
    wait_for(meta.at[0 : NY - 1], sent.at[6])
    wait_for(count.at[0 : nzc - 1, :, 0:4 * qk], sent.at[7])
    wait_for(count.at[0 : nzc - 1, :, 0:2 * qk], sent.at[8])
    wait_for(og.at[0 : n_tp * NC - 1], sent.at[9])
    wait_for(ag.at[0, 0, 0 : NY - 1], sent.at[10])
    wait_for(ag.at[0, 0 : nz - 1], sent.at[11])
    wait_for(ag.at[0], sent.at[12])
    wait_for(xg.at[0 : n_tp - 1], sent.at[13])
    wait_for(zg.at[0 : nz - 1], sent.at[14])
    wait_for(count.at[0 : nyc - 1, :, 0:share], sent.at[15])


def per_device(
    tokens,
    state_c,
    state_n,
    state_m,
    mix_gain,
    w_query,
    w_key,
    w_value,
    w_input_gate,
    w_forget_gate,
    forget_bias,
    w_output,
    moe_gain,
    w_group,
    expert_ids,
    expert_weight,
    w_exp_gate,
    w_exp_up,
    w_exp_down,
    w_dense,
    w_dense_gate,
):
    n_ep, n_tp = lax.axis_size("ep"), lax.axis_size("tp")
    nz = n_ep // (NY * NC)
    width = tokens.shape[1]
    rows = w_query.shape[0]
    block = NY * NC * rows
    lanes = min(128, block)
    share = width // n_tp
    nzc, nyc = nz * NC, NY * NC
    hidden = w_exp_gate.shape[2]
    qkv = 2 * w_query.shape[1] + w_value.shape[1]
    vm = pl.BlockSpec(memory_space=pltpu.VMEM)
    anywhere = pl.BlockSpec(memory_space=pl.ANY)
    V = pltpu.VMEM

    def kernel(*refs):
        layer_kernel(n_ep, n_tp, *refs)

    in_specs = [vm] * 21
    for k in (1, 16, 17, 18):
        in_specs[k] = anywhere
    out_shape = (
        jax.ShapeDtypeStruct((2, share), BF),
        jax.ShapeDtypeStruct(state_c.shape, F32),
        jax.ShapeDtypeStruct(state_n.shape, F32),
        jax.ShapeDtypeStruct(state_m.shape, F32),
    )
    scratch = [
        V((16, width), BF),
        V((2 * nzc, block), BF),
        V((2 * nzc, block), BF),
        V((16, 128), BF),
        V((NY, 2 * nzc, 128), BF),
        V((block, qkv), BF),
        V((block, w_output.shape[0]), BF),
        V((nz, lanes, share), BF),
        V((2 * nzc, qkv), BF),
        V((2 * nzc, qkv), BF),
        V(state_c.shape, F32),
        V(state_c.shape, F32),
        V((16, w_output.shape[0]), BF),
        V((2 * nzc, w_output.shape[0]), BF),
        V((2 * nzc, block), BF),
        V((n_tp * NC, 2 * nzc, block), BF),
        V((2 * nzc, block), BF),
        V((2, nz, NY, nzc, block), BF),
        V((2 * n_ep, width), BF),
        V((2 * nyc, width), BF),
        V((width, hidden), BF),
        V((width, hidden), BF),
        V((hidden, width), BF),
        V((n_tp, n_ep, share), BF),
        V((n_tp, n_ep, share), BF),
        V((n_ep, share), BF),
        V((nz, nyc, share), BF),
        V((2 * nyc, share), BF),
        V((2 * nyc, share), BF),
        pltpu.SemaphoreType.DMA((8,)),
        pltpu.SemaphoreType.DMA((16,)),
        pltpu.SemaphoreType.DMA((16,)),
        pltpu.SemaphoreType.DMA((nz,)),
        V((max(nzc, nyc), 2, qkv), BF),
    ]
    return pl.pallas_call(
        kernel,
        name="layer",
        out_shape=out_shape,
        in_specs=in_specs,
        out_specs=(vm, anywhere, vm, vm),
        scratch_shapes=scratch,
        compiler_params=pltpu.CompilerParams(
            collective_id=0, has_side_effects=True, vmem_limit_bytes=40 * 1024 * 1024
        ),
    )(
        tokens,
        state_c,
        state_n,
        state_m,
        mix_gain.reshape(1, -1),
        w_query,
        w_key,
        w_value,
        w_input_gate.T,
        w_forget_gate.T,
        forget_bias.reshape(1, -1),
        w_output.T,
        moe_gain.reshape(1, -1),
        w_group.T,
        expert_ids,
        expert_weight,
        w_exp_gate,
        w_exp_up,
        w_exp_down,
        w_dense,
        w_dense_gate.reshape(1, -1),
    )


def solution(mesh):
    placed = (
        P("ep", None),
        P("ep", "tp", None, None),
        P("ep", "tp", None),
        P("ep", "tp"),
        P(),
        P("ep", "tp"),
        P("ep", "tp"),
        P("ep", "tp"),
        P(),
        P(),
        P(),
        P("tp", "ep"),
        P(),
        P(),
        P("ep", None),
        P("ep", None),
        P("ep", None, "tp"),
        P("ep", None, "tp"),
        P("ep", "tp", None),
        P("ep", "tp"),
        P(),
    )
    return jax.shard_map(
        per_device,
        mesh=mesh,
        in_specs=placed,
        out_specs=(P("ep", "tp"), P("ep", "tp", None, None), P("ep", "tp", None), P("ep", "tp")),
        check_vma=False,
    )
```

time: 285 us -> 94.5 us (0.33)
  waiting for transfers between devices: 219 us -> 0 us
  Pallas kernels: 0 us -> 76.4 us
  starting transfers between devices: 24.3 us -> 0 us
  matrix products: 13.7 us -> 0 us
  between operations: 14 us -> 0.71 us
  local copies, waits for them, and re-layouts: 5.32 us -> 16.5 us
  other arithmetic: 7.77 us -> 0 us
    all_gather x3 -> x0, waiting for transfers between devices: 170 us -> none  [the longest x1 86.7 us: side_by_side(): lax.all_gather(both, axis, axis=dim, tiled=True)]
    pallas_call x0 -> x1, Pallas kernels: none -> 76.4 us  [per_device(): pl.pallas_call(kernel, name='layer', out_shape=out_shape, in_specs=in_spe...]
    all_to_all x4 -> x0, waiting for transfers between devices: 46.8 us -> none  [the longest x1 20.3 us: per_device(): lax.all_to_all(outgoing, 'ep', split_axis=0, concat_axis=0, tiled=True)]
    all_to_all x4 -> x0, starting transfers between devices: 24.2 us -> none  [the longest x1 11 us: per_device(): lax.all_to_all(outgoing, 'ep', split_axis=0, concat_axis=0, tiled=True)]
    dot_general x14 -> x0, matrix products: 13.7 us -> none  [the longest x3 4.91 us: per_device(): jnp.dot(feature_cols, weight_rows, preferred_element_type=jnp.float32)]
    unnamed x32 -> x44, local copies, waits for them, and re-layouts: 2.47 us -> 15.8 us
  transfers between devices with their start and end apart: 7 -> 0, of which waited for: 7 -> 0; matrix products, arithmetic and copies ran while one was open for 8% -> 0% of each run, Pallas kernels for 0% -> 0%
where the time goes in v1:
time: 94.5 us; the launch traced here: 93.6 us
  Pallas kernels  76.4 us (81%)
  local copies, waits for them, and re-layouts  16.5 us (17%)
    pallas_call x1, Pallas kernels, per_device(): pl.pallas_call(kernel, name='layer', out_shape=out_shape, in_specs=in_spe...  76.4 us
    unnamed x44, local copies, waits for them, and re-layouts  15.8 us

profile of v1, /device:TPU:1, one launch (start us, length us, event | category | flops | bytes accessed | tf_op | source)
XLA Modules:
  0.0 93.6 jit_solution(5919133109813414626)
XLA Ops:
  0.6 0.0 copy-start.6
  0.6 0.0 copy-start.10
  0.7 0.0 copy-start.16
  0.7 0.7 reshape.23.refs_20_
  1.4 0.0 copy-done.6
  1.4 0.0 copy-done.10
  1.4 0.0 copy-done.16
  1.4 0.0 copy-start
  1.4 1.0 %copy-done = f32[2,2,128,256]{3,2,1,0:T(8,128)S(1)} copy-done((f32[2,2,128,256]{3,2,1,0:T(8,128)S(1)}, f32[2,2,128,256]{3,2,1,0:T(8,128)}, u32[]{:S(2)}) %copy-start) | copy-done | bytes 524312
  2.4 0.0 copy-start.1
  2.4 1.0 %copy-done.1 = bf16[1,2048,128]{2,1,0:T(8,128)(2,1)S(1)} copy-done((bf16[1,2048,128]{2,1,0:T(8,128)(2,1)S(1)}, bf16[1,2048,128]{2,1,0:T(8,128)(2,1)}, u32[]{:S(2)}) %copy-start.1) | copy-done | bytes 524312
  3.5 0.0 copy-start.2
  3.5 1.0 %copy-done.2 = bf16[1,2048,128]{2,1,0:T(8,128)(2,1)S(1)} copy-done((bf16[1,2048,128]{2,1,0:T(8,128)(2,1)S(1)}, bf16[1,2048,128]{2,1,0:T(8,128)(2,1)}, u32[]{:S(2)}) %copy-start.2) | copy-done | bytes 524312
  4.5 0.0 copy-start.3
  4.5 1.0 %copy-done.3 = bf16[1,128,2048]{2,1,0:T(8,128)(2,1)S(1)} copy-done((bf16[1,128,2048]{2,1,0:T(8,128)(2,1)S(1)}, bf16[1,128,2048]{2,1,0:T(8,128)(2,1)}, u32[]{:S(2)}) %copy-start.3) | copy-done | bytes 524312
  5.6 0.0 copy-start.4
  5.6 0.8 copy-done.4
  6.3 0.0 copy-start.5
  6.3 0.8 copy-done.5
  7.1 0.0 copy-start.7
  7.1 0.7 copy-done.7
  7.8 0.0 copy-start.8
  7.8 0.7 copy-done.8
  8.5 0.0 copy-start.9
  8.5 0.7 copy-done.9
  9.2 0.0 copy-start.11
  9.2 0.7 copy-done.11
  9.9 0.0 copy-start.12
  9.9 0.7 copy-done.12
  10.6 0.0 copy-start.13
  10.6 0.7 copy-done.13
  11.3 0.0 copy-start.14
  11.3 0.7 copy-done.14
  12.0 0.0 copy-start.15
  12.0 0.7 copy-done.15
  12.7 0.0 copy-start.17
  12.7 0.7 copy-done.17
  13.4 0.0 copy-start.18
  13.4 0.7 copy-done.18
  14.1 0.0 copy-start.19
  14.1 0.7 copy-done.19
  14.7 76.4 %layer.1 = (bf16[2,512]{1,0:T(2,128)(2,1)S(1)}, f32[2,2,128,256]{3,2,1,0:T(8,128)S(1)}, f32[2,2,128]{2,1,0:T(2,128)S(1)}, f32[2,2]{1,0:T(2,128)S(1)}) custom-call(bf16[2,2048]{1,0:T(2,128)(2,1)S(1)} %copy-done.10, f32[2,2,128,256]{3,2,1,0:T(8,128)S(1)} %copy-done, f32[2,2,128]{2,1,0:T(2,128)S(1)} %copy-done.15, f32[2,2]{1,0:T(2,128)S(1)} %copy-done.16, ...), custom_call_target="tpu_custom_call" | custom-call | tf_op jit(solution)/shard_map/layer/pallas_call | solution.py:591
  91.1 0.6 copy.29
  91.7 0.8 copy.30
  92.5 0.6 copy.31
  93.1 0.6 copy.32
Async XLA Ops:
  0.6 0.7 copy-start.6
  0.6 0.7 copy-start.10
  0.7 0.7 copy-start.16
  1.4 1.0 %copy-start = (f32[2,2,128,256]{3,2,1,0:T(8,128)S(1)}, f32[2,2,128,256]{3,2,1,0:T(8,128)}, u32[]{:S(2)}) copy-start(f32[2,2,128,256]{3,2,1,0:T(8,128)} %refs_1_.1) | copy-start | bytes 1572868
  2.4 1.0 %copy-start.1 = (bf16[1,2048,128]{2,1,0:T(8,128)(2,1)S(1)}, bf16[1,2048,128]{2,1,0:T(8,128)(2,1)}, u32[]{:S(2)}) copy-start(bf16[1,2048,128]{2,1,0:T(8,128)(2,1)} %refs_16_.1) | copy-start | bytes 1572868
  3.5 1.0 %copy-start.2 = (bf16[1,2048,128]{2,1,0:T(8,128)(2,1)S(1)}, bf16[1,2048,128]{2,1,0:T(8,128)(2,1)}, u32[]{:S(2)}) copy-start(bf16[1,2048,128]{2,1,0:T(8,128)(2,1)} %refs_17_.1) | copy-start | bytes 1572868
  4.5 1.0 %copy-start.3 = (bf16[1,128,2048]{2,1,0:T(8,128)(2,1)S(1)}, bf16[1,128,2048]{2,1,0:T(8,128)(2,1)}, u32[]{:S(2)}) copy-start(bf16[1,128,2048]{2,1,0:T(8,128)(2,1)} %refs_18_.1) | copy-start | bytes 1572868
  5.6 0.8 copy-start.4
  6.3 0.8 copy-start.5
  7.1 0.7 copy-start.7
  7.8 0.7 copy-start.8
  8.5 0.7 copy-start.9
  9.2 0.7 copy-start.11
  9.9 0.7 copy-start.12
  10.6 0.7 copy-start.13
  11.3 0.7 copy-start.14
  12.0 0.7 copy-start.15
  12.7 0.7 copy-start.17
  13.4 0.7 copy-start.18
  14.1 0.7 copy-start.19

commit v2 on v1

v2 whole, which is shorter than its diff:
```python
import jax
import jax.numpy as jnp
from jax import lax
from jax.experimental import pallas as pl
from jax.experimental.pallas import tpu as pltpu
from jax.sharding import PartitionSpec as P

NY = 8
NC = 2
eps = 1e-06
BF = jnp.bfloat16
F32 = jnp.float32
MESH = pl.DeviceIdType.MESH
NN = (((1,), (0,)), ((), ()))
NT = (((1,), (1,)), ((), ()))
TN = (((0,), (0,)), ((), ()))


def mm(a, b, dims=NN, precision=None):
    return lax.dot_general(a, b, dims, precision=precision, preferred_element_type=F32)


def iota(shape, dim):
    return lax.broadcasted_iota(jnp.int32, shape, dim)


def ones_where(mask):
    return jnp.where(mask, 1.0, 0.0).astype(BF)


def each(count, body):
    def step(d, carry):
        body(d)
        return carry

    lax.fori_loop(1, count, step, 0)


def wait_for(ref, sem):
    pltpu.make_async_copy(ref, ref, sem).wait()


def layer_kernel(
    n_ep,
    n_tp,
    tokens_h,
    state_c_h,
    state_n_h,
    state_m_h,
    mix_gain_h,
    w_query_h,
    w_key_h,
    w_value_h,
    w_in_h,
    w_forget_h,
    forget_bias_h,
    w_out_h,
    moe_gain_h,
    w_group_h,
    expert_ids_h,
    expert_weight_h,
    w_gate_h,
    w_up_h,
    w_down_h,
    w_dense_h,
    w_dense_gate_h,
    mixed,
    new_c,
    new_n,
    new_m,
    nrm,
    nrmh,
    tn,
    tny,
    tr,
    meta_own,
    meta,
    wqk,
    wv,
    wot,
    wd,
    pb,
    rb,
    pbv,
    rbv,
    c_in,
    c_out,
    hb,
    hg,
    op,
    og,
    ag,
    n2,
    hidden,
    meta_rows,
    n2z,
    wg,
    wu,
    wdn,
    dp,
    xg,
    eo,
    zg,
    ys,
    yg,
    loads,
    sent,
    got,
    got_z,
    got_far,
    got_y,
    got_x,
    count,
    tokens,
    state_n,
    state_m,
    mix_gain,
    w_in,
    w_forget,
    forget_bias,
    moe_gain,
    w_group,
    expert_ids,
    expert_weight,
    w_dense_gate,
):
    nz = n_ep // (NY * NC)
    rows = w_query_h.shape[0]
    width = tokens.shape[1]
    block = NY * NC * rows
    nzc, nyc = nz * NC, NY * NC
    half = nz * NC
    seqs = 2 * n_ep
    share = width // n_tp
    qk = w_query_h.shape[1]
    lanes = wd.shape[1]
    group_count = w_group.shape[0]

    ep = lax.axis_index("ep")
    x = lax.axis_index("tp")
    z = ep // nyc
    y = (ep // NC) % NY
    c = ep % NC
    zc = z * NC + c
    yc = y * NC + c

    def device(z_, y_, c_, x_):
        return {"ep": (z_ * NY + y_) * NC + c_, "tp": x_}

    def send(src, dst, s, r, to):
        pltpu.make_async_remote_copy(
            src_ref=src, dst_ref=dst, send_sem=s, recv_sem=r, device_id=to, device_id_type=MESH
        ).start()

    def y_peer(d):
        return device(z, (y + d) % NY, c, x)

    def zc_peer(d):
        other = (zc + d) % nzc
        return other // NC, other, device(other // NC, y, other % NC, x)

    def yc_peer(d):
        other = (yc + d) % nyc
        return other, device(z, other // NC, other % NC, x)

    def xc_peer(d):
        other = (x * NC + c + d) % (n_tp * NC)
        return device(z, y, other % NC, other // NC)

    started = {}

    def load(name, src, dst):
        started[name] = pltpu.make_async_copy(src, dst, loads.at[8 + len(started)])
        started[name].start()

    load("tokens", tokens_h, tokens)
    load("mix_gain", mix_gain_h, mix_gain)
    load("expert_ids", expert_ids_h, expert_ids)
    load("expert_weight", expert_weight_h, expert_weight)

    wqk[...] = jnp.zeros_like(wqk)
    wv[...] = jnp.zeros_like(wv)
    wot[...] = jnp.zeros_like(wot)
    wd[...] = jnp.zeros_like(wd)
    own = pl.ds(pl.multiple_of(yc * rows, rows), rows)
    start = yc * rows
    dense_block = start // lanes
    dense_rows = pl.ds(pl.multiple_of(start % lanes, rows), rows)
    load("w_query", w_query_h, wqk.at[own, 0:qk])
    load("w_key", w_key_h, wqk.at[own, qk : 2 * qk])
    load("w_value", w_value_h, wv.at[z, dense_rows, :])
    load("w_out", w_out_h, wot.at[own, :])
    load("w_dense", w_dense_h, wd.at[z, dense_rows, :])
    load("w_in", w_in_h, w_in)
    load("w_forget", w_forget_h, w_forget)
    load("forget_bias", forget_bias_h, forget_bias)
    load("state_m", state_m_h, state_m)
    load("state_n", state_n_h, state_n)
    load("state_c", state_c_h, c_in)
    load("moe_gain", moe_gain_h, moe_gain)
    load("w_group", w_group_h, w_group)
    load("w_dense_gate", w_dense_gate_h, w_dense_gate)
    load("w_gate", w_gate_h.at[0], wg)
    load("w_up", w_up_h.at[0], wu)
    load("w_down", w_down_h.at[0], wdn)

    def loaded(*names):
        for name in names:
            started[name].wait()

    barrier = pltpu.get_barrier_semaphore()

    def greet(to):
        pl.semaphore_signal(barrier, inc=1, device_id=to, device_id_type=MESH)

    each(nyc, lambda d: greet(yc_peer(d)[1]))
    each(nzc, lambda d: greet(zc_peer(d)[2]))
    each(n_tp * NC, lambda d: greet(xc_peer(d)))

    loaded("tokens", "mix_gain", "expert_ids", "expert_weight")
    wide = tokens[...].astype(F32)
    inverse = lax.rsqrt(jnp.mean(wide * wide, axis=-1, keepdims=True) + eps)
    nrm[...] = jnp.zeros_like(nrm)
    normed = (wide * inverse * mix_gain[...]).astype(BF)
    nrm[0:2, :] = normed
    for k in range(block // lanes):
        for b in range(nz):
            first = b * block + k * lanes
            nrmh[k, 0:2, b * lanes : (b + 1) * lanes] = normed[:, first : first + lanes]
    lane = iota((2, 128), 1)
    idf = expert_ids[...].astype(F32)
    ewt = expert_weight[...]
    ew_hi = ewt.astype(BF).astype(F32)
    ew_lo = ewt - ew_hi
    packed = jnp.zeros((2, 128), F32)
    for k, part in enumerate((idf, ew_hi, ew_lo)):
        for j in range(2):
            packed = jnp.where(lane == 2 * k + j, part[:, j : j + 1], packed)
    meta_own[...] = jnp.zeros_like(meta_own)
    meta_own[0:2, :] = packed.astype(BF)

    loaded("w_query", "w_key", "w_value", "w_out", "w_dense")
    pl.semaphore_wait(barrier, (nyc - 1) + (nzc - 1) + (n_tp * NC - 1))

    def pair(index):
        return pl.ds(pl.multiple_of(2 * index, 2), 2)

    def cols(index):
        return pl.ds(pl.multiple_of(index * block, block), block)

    def send_rows(d):
        z_, _, to = zc_peer(d)
        send(nrm.at[0:2, cols(z_)], tn.at[pair(zc), :], sent.at[1], got.at[1], to)

    def send_raw(d):
        z_, _, to = zc_peer(d)
        send(tokens.at[:, cols(z_)], tr.at[pair(zc), :], sent.at[2], got.at[2], to)
        send(meta_own.at[0:2, :], meta.at[y, pair(zc), :], sent.at[3], got.at[3], to)

    def half_of(index):
        return nrmh.at[(index * rows) // lanes, 0:2, :]

    def send_halves(d):
        other, to = yc_peer(d)
        send(half_of(other), tny.at[pair(yc), :], sent.at[16], got.at[16], to)

    def z_peer(d):
        return device((z + d) % nz, y, c, x)

    mine_p, mine_o = wqk.at[own, :], wot.at[own, :]
    mine_v, mine_d = wv.at[z, dense_rows, :], wd.at[z, dense_rows, :]
    each(NY, lambda d: send(mine_p, mine_p, sent.at[0], got.at[0], y_peer(d)))
    each(nz, lambda d: send(mine_v, mine_v, sent.at[17], got.at[17], z_peer(d)))
    each(nzc, send_rows)
    each(nyc, send_halves)
    each(NY, lambda d: send(mine_o, mine_o, sent.at[4], got.at[4], y_peer(d)))
    each(nzc, send_raw)
    each(
        nz,
        lambda d: send(
            mine_d,
            mine_d,
            sent.at[5],
            got.at[5],
            z_peer(d),
        ),
    )
    keep_v = pltpu.make_async_copy(half_of(yc), tny.at[pair(yc), :], loads.at[3])
    keep_v.start()
    keep_n = pltpu.make_async_copy(nrm.at[0:2, cols(z)], tn.at[pair(zc), :], loads.at[4])
    keep_r = pltpu.make_async_copy(tokens.at[:, cols(z)], tr.at[pair(zc), :], loads.at[7])
    keep_m = pltpu.make_async_copy(meta_own.at[0:2, :], meta.at[y, pair(zc), :], loads.at[6])
    for copy in (keep_n, keep_r, keep_m):
        copy.start()

    loaded("w_in", "w_forget", "forget_bias", "state_m")
    head_count = state_m.shape[1]
    gate_all = mm(nrm[...], w_in[...], NT)[0:2]
    raw = mm(nrm[...], w_forget[...], NT)[0:2] + forget_bias[...]
    forget_all = jnp.minimum(raw, 0.0) - jnp.log1p(jnp.exp(-jnp.abs(raw)))
    head_lane = iota(gate_all.shape, 1)

    def of_head(values, h):
        mine = head_lane == x * head_count + h
        return jnp.sum(jnp.where(mine, values, 0.0), axis=1, keepdims=True)

    decays, inflows, ms = [], [], []
    for h in range(head_count):
        gate_h, forget_h = of_head(gate_all, h), of_head(forget_all, h)
        kept = forget_h + state_m[:, h : h + 1]
        m_h = jnp.maximum(kept, gate_h)
        decays.append(jnp.exp(kept - m_h))
        inflows.append(jnp.exp(gate_h - m_h))
        ms.append(m_h)
    m_lane = iota(state_m.shape, 1)
    new_m_value = jnp.zeros(state_m.shape, F32)
    for h in range(head_count):
        new_m_value = jnp.where(m_lane == h, ms[h], new_m_value)
    new_m[...] = new_m_value

    keep_n.wait()
    wait_for(count.at[0 : nzc - 1, :, 0:block], got.at[1])
    wait_for(wqk.at[0 : (NY - 1) * rows, :], got.at[0])
    pb[...] = mm(tn[...], wqk[...]).astype(BF)
    keep_p = pltpu.make_async_copy(pb.at[pair(zc), :], rb.at[pair(zc), :], loads.at[4])
    keep_p.start()

    def send_partial(d):
        _, other, to = zc_peer(d)
        send(pb.at[pair(other), :], rb.at[pair(zc), :], sent.at[7], got.at[7], to)

    each(nzc, send_partial)
    keep_v.wait()
    wait_for(count.at[0 : nyc - 1, :, 0 : nz * lanes], got.at[16])
    wait_for(wv.at[0 : nz - 1, 0:rows, :], got.at[17])
    pbv[...] = mm(tny[...], wv[...].reshape(nz * lanes, -1)).astype(BF)
    keep_v = pltpu.make_async_copy(pbv.at[pair(yc), :], rbv.at[pair(yc), :], loads.at[3])
    keep_v.start()

    def send_partial_v(d):
        other, to = yc_peer(d)
        send(pbv.at[pair(other), :], rbv.at[pair(yc), :], sent.at[18], got.at[18], to)

    each(nyc, send_partial_v)
    keep_m.wait()
    wait_for(count.at[0 : nzc - 1, :, 0:128], got.at[3])
    each(NY, lambda d: send(meta.at[y], meta.at[y], sent.at[6], got.at[6], y_peer(d)))

    loaded("state_c", "state_n")
    keep_p.wait()
    wait_for(count.at[0 : nzc - 1, :, 0 : 2 * qk], got.at[7])
    keep_v.wait()
    wait_for(count.at[0 : nyc - 1, :, 0 : 2 * qk], got.at[18])

    def pair_sum(count):
        r, col = iota((16, 2 * count), 0), iota((16, 2 * count), 1)
        return ones_where((col & 1) == r)

    rows_qk = mm(pair_sum(nzc), rb[...]).astype(BF)
    rows_v = mm(pair_sum(nyc), rbv[...]).astype(BF)

    row = iota((16, 1), 0)
    dqk, dv = c_in.shape[2], c_in.shape[3]
    for h in range(head_count):
        q = rows_qk[:, h * dqk : (h + 1) * dqk]
        k = rows_qk[:, qk + h * dqk : qk + (h + 1) * dqk]
        v = rows_v[:, h * dv : (h + 1) * dv]
        qf, kf = q.astype(F32), k.astype(F32)
        heads = jnp.zeros((16, dv), F32)
        for t in range(2):
            decay = decays[h][t : t + 1, :]
            inflow = inflows[h][t : t + 1, :] * dqk ** (-0.5)
            outer = mm(jnp.where(row == t, kf, 0.0).astype(BF), v, TN)
            c_new = decay * c_in[t, h] + inflow * outer
            c_out[t, h] = c_new
            n_new = decay * state_n[t, h : h + 1, :] + inflow * kf[t : t + 1, :]
            new_n[t, h : h + 1, :] = n_new
            numer = mm(qf, c_new, precision=lax.Precision.HIGHEST)
            denom = jnp.sum(qf[t : t + 1, :] * n_new, axis=-1, keepdims=True)
            denom = jnp.maximum(jnp.abs(denom), 1.0)
            heads = jnp.where(row == t, numer / denom, heads)
        hb[:, h * dv : (h + 1) * dv] = heads.astype(BF)

    store_c = pltpu.make_async_copy(c_out, new_c, loads.at[5])
    store_c.start()

    keep_h = pltpu.make_async_copy(hb.at[0:2, :], hg.at[pair(zc), :], loads.at[4])
    keep_h.start()
    each(
        nzc,
        lambda d: send(
            hb.at[0:2, :], hg.at[pair(zc), :], sent.at[8], got.at[8], zc_peer(d)[2]
        ),
    )
    wait_for(wot.at[0 : (NY - 1) * rows, :], got.at[4])
    keep_r.wait()
    wait_for(count.at[0 : nzc - 1, :, 0:block], got.at[2])
    keep_h.wait()
    wait_for(count.at[0 : nzc - 1, :, 0 : 2 * qk], got.at[8])
    op[...] = mm(hg[...], wot[...], NT).astype(BF)
    xc = x * NC + c

    def half_rows(c_):
        return pl.ds(pl.multiple_of(c_ * half, half), half)

    def send_parts(d):
        other = (xc + d) % (n_tp * NC)
        to = device(z, y, other % NC, other // NC)
        send(op.at[half_rows(other % NC), :], og.at[xc], sent.at[9], got.at[9], to)

    each(n_tp * NC, send_parts)
    og[xc] = op[half_rows(c), :]
    wait_for(og.at[0 : n_tp * NC - 1], got.at[9])
    parts = jnp.zeros((half, block), F32)
    for k in range(n_tp * NC):
        parts = parts + og[k].astype(F32)

    sa = z + c * (y - z)
    sb = y + c * (z - y)

    def at(a, b):
        return device(a + c * (b - a), b + c * (a - b), c, x)

    ag[c, sa, sb] = (tr[half_rows(c), :].astype(F32) + parts).astype(BF)
    mine = ag.at[c, sa, sb]
    partner = device(z, y, 1 - c, x)
    near = 2 * min(2, (NY - 1) // 2)
    ring = sorted(range(1, NY), key=lambda d: min(d, NY - d))

    def spread(ref, r):
        for d in sorted(range(1, nz), key=lambda d: -min(d, nz - d)):
            send(ref, ref, sent.at[11], r.at[d], at((sa + d) % nz, sb))

    for d in ring:
        send(mine, mine, sent.at[10], got_y.at[d], at(sa, (sb + d) % NY))
    spread(mine, got_z)
    for index, d in enumerate(ring):
        block_in = ag.at[c, sa, (sb + NY - d) % NY]
        wait_for(block_in, got_y.at[d])
        spread(block_in, got_z if index < near else got_far)

    def swap(ref):
        send(ref, ref, sent.at[12], got.at[11], partner)

    swap(ag.at[c, sa])
    lines = sorted(range(1, nz), key=lambda d: min(d, nz - d))
    for d in lines:
        wait_for(ag.at[0, 0, 0 : near + 1], got_z.at[d])
        wait_for(ag.at[0, 0, near + 1 : NY], got_far.at[d])
        swap(ag.at[c, (sa + nz - d) % nz])
    wait_for(meta.at[0 : NY - 1], got.at[6])
    loaded("moe_gain", "w_group", "w_dense_gate", "w_gate", "w_up", "w_down")
    side = seqs // 2

    def rows_of(h, b):
        pieces = [ag[h, b + h * (k - b), k + h * (b - k)] for k in range(NY)]
        return jnp.concatenate(pieces, axis=0)

    expert = ep.astype(F32)

    def run_half(h):
        squares = jnp.zeros((side, block), F32)
        for b in range(nz):
            piece = rows_of(h, b).astype(F32)
            squares = squares + piece * piece
        mean = jnp.sum(squares, axis=-1, keepdims=True) * (1.0 / width)
        inverse = lax.rsqrt(mean + eps)
        at_rows = pl.ds(pl.multiple_of(h * side, side), side)
        for b in range(nz):
            piece = rows_of(h, b).astype(F32)
            gain = moe_gain[:, b * block : (b + 1) * block]
            n2[at_rows, b * block : (b + 1) * block] = (piece * inverse * gain).astype(BF)
        gate_act = mm(n2[at_rows, :], wg[...])
        up_act = mm(n2[at_rows, :], wu[...])
        act = gate_act * jax.nn.sigmoid(gate_act) * up_act
        facts = meta[:, half_rows(h), :].reshape(side, 128)
        meta_rows[at_rows, :] = facts
        ids = facts.astype(F32)
        assigned = (ids[:, 0:1] == expert) | (ids[:, 1:2] == expert)
        hidden[at_rows, :] = jnp.where(assigned, act, 0.0).astype(BF)

    run_half(c)
    wait_for(ag.at[0], got.at[11])
    run_half(1 - c)

    def token_of(shape):
        r = iota(shape, 1)
        h, y_, rest = r // side, (r // half) % NY, r % half
        z_ = h * (nz // 2) + rest // (2 * NC)
        return ((z_ * NY + y_) * NC) * 2 + rest % (2 * NC)

    slot_rows = iota((n_ep, seqs), 0)
    placing = ones_where(token_of((n_ep, seqs)) // 2 == slot_rows)
    slots = mm(placing, hidden[...]).astype(BF)

    def down(x_):
        return mm(slots, wdn[:, pl.ds(pl.multiple_of(x_ * share, share), share)]).astype(BF)

    for d in range(1, n_tp):
        dp[d] = down((x + d) % n_tp)
    order = sorted(range(nz), key=lambda k: -min(k, nz - k))

    def rows_at(k):
        return pl.ds(pl.multiple_of(((z + k) % nz) * nyc, nyc), nyc)

    for k in order:
        for d in sorted(range(1, n_tp), key=lambda d: -min(d, n_tp - d)):
            to = device(z, y, c, (x + d) % n_tp)
            send(dp.at[d, rows_at(k)], xg.at[x, rows_at(k)], sent.at[13], got_x.at[k], to)
    xg[x] = down(x)

    local = ones_where(token_of((2 * nyc, seqs)) == z * 2 * nyc + iota((2 * nyc, seqs), 0))
    picks = mm(local, meta_rows[...])
    zrows = mm(local, n2[...]).astype(BF)
    n2z[...] = zrows
    wait_for(wd.at[0 : nz - 1, 0:rows, :], got.at[5])
    dense = jnp.zeros((2 * nyc, share), F32)
    for b in range(nz):
        at_lane = pl.multiple_of(b * block + dense_block * lanes, lanes)
        dense = dense + mm(n2z[:, pl.ds(at_lane, lanes)], wd[b])
    gate_rows = w_dense_gate[...].astype(F32)
    products = jnp.zeros((2 * nyc, 128), F32)
    for k in range(width // 128):
        at_cols = slice(k * 128, (k + 1) * 128)
        products = products + zrows[:, at_cols].astype(F32) * gate_rows[k : k + 1, :]
    dense_gate = jnp.sum(products, axis=-1, keepdims=True)
    dense = jax.nn.sigmoid(dense_gate) * dense
    logits = mm(zrows, w_group[...], NT)
    shifted = jnp.exp(logits - jnp.max(logits, axis=-1, keepdims=True))
    prob = shifted / jnp.sum(shifted, axis=-1, keepdims=True)
    per_group = n_ep // group_count
    first = (iota(prob.shape, 1) * per_group).astype(F32)
    weights = [picks[:, 2 + j : 3 + j] + picks[:, 4 + j : 5 + j] for j in range(2)]
    total = weights[0] + weights[1]
    at_slot = iota((2 * nyc, n_ep), 1)
    source = ((at_slot // nyc) * nyc + yc).astype(F32)
    same = at_slot % nyc == iota((2 * nyc, n_ep), 0) // 2
    mixing = jnp.zeros((2 * nyc, n_ep), F32)
    for j in range(2):
        ident = picks[:, j : j + 1]
        member = (ident >= first) & (ident < first + per_group)
        picked = jnp.sum(jnp.where(member, prob, 0.0), axis=-1, keepdims=True)
        route = picked * weights[j] / total
        mixing = mixing + jnp.where(same & (ident == source), route, 0.0)
    mix_hi = mixing.astype(BF)
    mix_lo = (mixing - mix_hi.astype(F32)).astype(BF)
    owned = ones_where(
        (token_of((16, seqs)) == 2 * ep + iota((16, seqs), 0)) & (iota((16, seqs), 0) < 2)
    )
    per_share = nz // n_tp
    residual = []
    for k in range(per_share):
        b = x * per_share + k
        residual.append(
            mm(owned[:, 0:side], ag[0, b].reshape(side, block))
            + mm(owned[:, side:], ag[1, :, b].reshape(side, block))
        )

    for k in order:
        wait_for(xg.at[0 : n_tp - 1, 0:nyc, :], got_x.at[k])
        total_out = xg[0, rows_at(k), :].astype(F32)
        for j in range(1, n_tp):
            total_out = total_out + xg[j, rows_at(k), :].astype(F32)
        if k == 0:
            zg[z] = total_out.astype(BF)
        else:
            eo[rows_at(k), :] = total_out.astype(BF)
            send(eo.at[rows_at(k), :], zg.at[z], sent.at[14], got.at[13], z_peer(k))
    wait_for(zg.at[0 : nz - 1], got.at[13])
    arrived = zg[...].reshape(n_ep, share)
    ys[...] = (mm(mix_hi, arrived) + mm(mix_lo, arrived) + dense).astype(BF)
    keep_y = pltpu.make_async_copy(ys.at[pair(yc), :], yg.at[pair(yc), :], loads.at[4])
    keep_y.start()

    def send_sums(d):
        other, to = yc_peer(d)
        send(ys.at[pair(other), :], yg.at[pair(yc), :], sent.at[15], got.at[14], to)

    each(nyc, send_sums)
    keep_y.wait()
    wait_for(count.at[0 : nyc - 1, :, 0:share], got.at[14])
    summed = mm(pair_sum(nyc), yg[...])
    for k in range(per_share):
        at_cols = slice(k * block, (k + 1) * block)
        mixed[:, at_cols] = (residual[k] + summed[:, at_cols])[0:2].astype(BF)

    store_c.wait()
    wait_for(wqk.at[0 : (NY - 1) * rows, :], sent.at[0])
    wait_for(count.at[0 : nyc - 1, :, 0 : nz * lanes], sent.at[16])
    wait_for(wv.at[0 : nz - 1, 0:rows, :], sent.at[17])
    wait_for(count.at[0 : nyc - 1, :, 0 : 2 * qk], sent.at[18])
    wait_for(count.at[0 : nzc - 1, :, 0:block], sent.at[1])
    wait_for(count.at[0 : nzc - 1, :, 0:block], sent.at[2])
    wait_for(count.at[0 : nzc - 1, :, 0:128], sent.at[3])
    wait_for(wot.at[0 : (NY - 1) * rows, :], sent.at[4])
    wait_for(wd.at[0 : nz - 1, 0:rows, :], sent.at[5])
    wait_for(meta.at[0 : NY - 1], sent.at[6])
    wait_for(count.at[0 : nzc - 1, :, 0 : 2 * qk], sent.at[7])
    wait_for(count.at[0 : nzc - 1, :, 0 : 2 * qk], sent.at[8])
    wait_for(og.at[0 : n_tp * NC - 1], sent.at[9])
    wait_for(ag.at[0, 0, 0 : NY - 1], sent.at[10])
    wait_for(ag.at[0, 0 : nz - 1], sent.at[11])
    wait_for(ag.at[0], sent.at[12])
    wait_for(xg.at[0 : n_tp - 1], sent.at[13])
    wait_for(zg.at[0 : nz - 1], sent.at[14])
    wait_for(count.at[0 : nyc - 1, :, 0:share], sent.at[15])


def per_device(
    tokens,
    state_c,
    state_n,
    state_m,
    mix_gain,
    w_query,
    w_key,
    w_value,
    w_input_gate,
    w_forget_gate,
    forget_bias,
    w_output,
    moe_gain,
    w_group,
    expert_ids,
    expert_weight,
    w_exp_gate,
    w_exp_up,
    w_exp_down,
    w_dense,
    w_dense_gate,
):
    n_ep, n_tp = lax.axis_size("ep"), lax.axis_size("tp")
    nz = n_ep // (NY * NC)
    width = tokens.shape[1]
    rows = w_query.shape[0]
    block = NY * NC * rows
    lanes = min(128, block)
    share = width // n_tp
    nzc, nyc = nz * NC, NY * NC
    hidden = w_exp_gate.shape[2]
    qkv = 2 * w_query.shape[1] + w_value.shape[1]
    vm = pl.BlockSpec(memory_space=pltpu.VMEM)
    anywhere = pl.BlockSpec(memory_space=pltpu.HBM)
    V = pltpu.VMEM

    def kernel(*refs):
        layer_kernel(n_ep, n_tp, *refs)

    in_specs = [anywhere] * 21
    out_shape = (
        jax.ShapeDtypeStruct((2, share), BF),
        jax.ShapeDtypeStruct(state_c.shape, F32),
        jax.ShapeDtypeStruct(state_n.shape, F32),
        jax.ShapeDtypeStruct(state_m.shape, F32),
    )
    scratch = [
        V((16, width), BF),
        V((block // lanes, 16, nz * lanes), BF),
        V((2 * nzc, block), BF),
        V((2 * nyc, nz * lanes), BF),
        V((2 * nzc, block), BF),
        V((16, 128), BF),
        V((NY, 2 * nzc, 128), BF),
        V((block, 2 * w_query.shape[1]), BF),
        V((nz, lanes, w_value.shape[1]), BF),
        V((block, w_output.shape[0]), BF),
        V((nz, lanes, share), BF),
        V((2 * nzc, 2 * w_query.shape[1]), BF),
        V((2 * nzc, 2 * w_query.shape[1]), BF),
        V((2 * nyc, w_value.shape[1]), BF),
        V((2 * nyc, w_value.shape[1]), BF),
        V(state_c.shape, F32),
        V(state_c.shape, F32),
        V((16, w_output.shape[0]), BF),
        V((2 * nzc, w_output.shape[0]), BF),
        V((2 * nzc, block), BF),
        V((n_tp * NC, nzc, block), BF),
        V((2, nz, NY, nzc, block), BF),
        V((2 * n_ep, width), BF),
        V((2 * n_ep, hidden), BF),
        V((2 * n_ep, 128), BF),
        V((2 * nyc, width), BF),
        V((width, hidden), BF),
        V((width, hidden), BF),
        V((hidden, width), BF),
        V((n_tp, n_ep, share), BF),
        V((n_tp, n_ep, share), BF),
        V((n_ep, share), BF),
        V((nz, nyc, share), BF),
        V((2 * nyc, share), BF),
        V((2 * nyc, share), BF),
        pltpu.SemaphoreType.DMA((32,)),
        pltpu.SemaphoreType.DMA((20,)),
        pltpu.SemaphoreType.DMA((20,)),
        pltpu.SemaphoreType.DMA((nz,)),
        pltpu.SemaphoreType.DMA((nz,)),
        pltpu.SemaphoreType.DMA((NY,)),
        pltpu.SemaphoreType.DMA((nz,)),
        V((max(nzc, nyc), 2, qkv), BF),
        V(tokens.shape, BF),
        V(state_n.shape, F32),
        V(state_m.shape, F32),
        V((1, width), F32),
        V(w_input_gate.shape[::-1], BF),
        V(w_forget_gate.shape[::-1], BF),
        V((1, forget_bias.shape[0]), F32),
        V((1, width), F32),
        V(w_group.shape[::-1], BF),
        V(expert_ids.shape, jnp.int32),
        V(expert_weight.shape, F32),
        V((width // 128, 128), BF),
    ]
    results = pl.pallas_call(
        kernel,
        name="layer",
        out_shape=out_shape,
        in_specs=in_specs,
        out_specs=(vm, anywhere, vm, vm),
        scratch_shapes=scratch,
        compiler_params=pltpu.CompilerParams(
            collective_id=0, has_side_effects=True, vmem_limit_bytes=67043328
        ),
    )(
        tokens,
        state_c,
        state_n,
        state_m,
        mix_gain.reshape(1, -1),
        w_query,
        w_key,
        w_value,
        w_input_gate.T,
        w_forget_gate.T,
        forget_bias.reshape(1, -1),
        w_output.T,
        moe_gain.reshape(1, -1),
        w_group.T,
        expert_ids,
        expert_weight,
        w_exp_gate,
        w_exp_up,
        w_exp_down,
        w_dense,
        w_dense_gate.reshape(-1, 128),
    )
    return pl.pallas_call(
        store_kernel,
        name="store",
        out_shape=out_shape,
        in_specs=[anywhere] * 4,
        out_specs=(anywhere,) * 4,
        scratch_shapes=[V(r.shape, r.dtype) for r in out_shape] + [pltpu.SemaphoreType.DMA((2, 4))],
        compiler_params=pltpu.CompilerParams(vmem_limit_bytes=67043328),
    )(*results)


def store_kernel(*refs):
    ins, outs, held, sems = refs[0:4], refs[4:8], refs[8:12], refs[12]
    order = (1, 0, 2, 3)
    for k in order:
        pltpu.make_async_copy(ins[k], held[k], sems.at[0, k]).start()
    for k in order:
        pltpu.make_async_copy(ins[k], held[k], sems.at[0, k]).wait()
        pltpu.make_async_copy(held[k], outs[k], sems.at[1, k]).start()
    for k in order:
        pltpu.make_async_copy(held[k], outs[k], sems.at[1, k]).wait()


def solution(mesh):
    placed = (
        P("ep", None),
        P("ep", "tp", None, None),
        P("ep", "tp", None),
        P("ep", "tp"),
        P(),
        P("ep", "tp"),
        P("ep", "tp"),
        P("ep", "tp"),
        P(),
        P(),
        P(),
        P("tp", "ep"),
        P(),
        P(),
        P("ep", None),
        P("ep", None),
        P("ep", None, "tp"),
        P("ep", None, "tp"),
        P("ep", "tp", None),
        P("ep", "tp"),
        P(),
    )
    return jax.shard_map(
        per_device,
        mesh=mesh,
        in_specs=placed,
        out_specs=(P("ep", "tp"), P("ep", "tp", None, None), P("ep", "tp", None), P("ep", "tp")),
        check_vma=False,
    )
```

time: 94.5 us -> 73.1 us (0.77)
  local copies, waits for them, and re-layouts: 16.5 us -> 0 us
  Pallas kernels: 76.4 us -> 72.3 us
    unnamed x44 -> x0, local copies, waits for them, and re-layouts: 15.8 us -> none
    pallas_call x1, Pallas kernels: 76.4 us -> 70.4 us  [per_device(): pl.pallas_call(kernel, name='layer', out_shape=out_shape, in_specs=in_spe...]
    pallas_call x0 -> x1, Pallas kernels: none -> 1.91 us  [per_device(): pl.pallas_call(store_kernel, name='store', out_shape=out_shape, in_specs=...]
where the time goes in v2:
time: 73.1 us; the launch traced here: 72.9 us
  Pallas kernels  72.3 us (99%)
    pallas_call x1, Pallas kernels, per_device(): pl.pallas_call(kernel, name='layer', out_shape=out_shape, in_specs=in_spe...  70.4 us
    pallas_call x1, Pallas kernels, per_device(): pl.pallas_call(store_kernel, name='store', out_shape=out_shape, in_specs=...  1.91 us

profile of v2, /device:TPU:1, one launch (start us, length us, event | category | flops | bytes accessed | tf_op | source)
XLA Modules:
  0.0 72.9 jit_solution(1826101186884212533)
XLA Ops:
  0.6 70.4 %layer.1 = (bf16[2,512]{1,0:T(2,128)(2,1)}, f32[2,2,128,256]{3,2,1,0:T(8,128)}, f32[2,2,128]{2,1,0:T(2,128)}, f32[2,2]{1,0:T(2,128)}) custom-call(bf16[2,2048]{1,0:T(2,128)(2,1)} %refs_0_.1, f32[2,2,128,256]{3,2,1,0:T(8,128)} %refs_1_.1, f32[2,2,128]{2,1,0:T(2,128)} %refs_2_.1, f32[2,2]{1,0:T(2,128)} %refs_3_.1, f32[1,2048]{1,0:T(1,128)} %bitcast.12, ...), custom_call_target="tpu_custom_call" | custom-call | tf_op jit(solution)/shard_map/layer/pallas_call | solution.py:713
  71.0 1.9 %store.1 = (bf16[2,512]{1,0:T(2,128)(2,1)}, f32[2,2,128,256]{3,2,1,0:T(8,128)}, f32[2,2,128]{2,1,0:T(2,128)}, f32[2,2]{1,0:T(2,128)}) custom-call(bf16[2,512]{1,0:T(2,128)(2,1)} %get-tuple-element.8.refs_0_, f32[2,2,128,256]{3,2,1,0:T(8,128)} %get-tuple-element.9.refs_1_, f32[2,2,128]{2,1,0:T(2,128)} %get-tuple-element.10.refs_2_, ...), custom_call_target="tpu_custom_call" | custom-call | tf_op jit(solution)/shard_map/store/pallas_call | solution.py:746

commit v3 on v2

--- a/solution.py
+++ b/solution.py
@@ -29,11 +29,12 @@
 
 
 def each(count, body):
-    def step(d, carry):
-        body(d)
+    def step(i, carry):
+        away = lax.div(i + 1, 2)
+        body(count // 2 + away - 2 * lax.rem(i, 2) * away)
         return carry
 
-    lax.fori_loop(1, count, step, 0)
+    lax.fori_loop(0, count - 1, step, 0)
 
 
 def wait_for(ref, sem):
@@ -85,13 +86,15 @@
     rbv,
     c_in,
     c_out,
+    n_out,
+    m_out,
+    mixed_out,
     hb,
     hg,
     op,
     og,
     ag,
     n2,
-    hidden,
     meta_rows,
     n2z,
     wg,
@@ -138,9 +141,9 @@
 
     ep = lax.axis_index("ep")
     x = lax.axis_index("tp")
-    z = ep // nyc
-    y = (ep // NC) % NY
-    c = ep % NC
+    z = lax.div(ep, nyc)
+    y = lax.rem(lax.div(ep, NC), NY)
+    c = lax.rem(ep, NC)
     zc = z * NC + c
     yc = y * NC + c
 
@@ -153,19 +156,34 @@
         ).start()
 
     def y_peer(d):
-        return device(z, (y + d) % NY, c, x)
+        return device(z, lax.rem(y + d, NY), c, x)
 
     def zc_peer(d):
-        other = (zc + d) % nzc
-        return other // NC, other, device(other // NC, y, other % NC, x)
+        other = lax.rem(zc + d, nzc)
+        z_ = lax.div(other, NC)
+        return z_, other, device(z_, y, lax.rem(other, NC), x)
 
     def yc_peer(d):
-        other = (yc + d) % nyc
-        return other, device(z, other // NC, other % NC, x)
+        other = lax.rem(yc + d, nyc)
+        return other, {"ep": z * nyc + other, "tp": x}
 
     def xc_peer(d):
-        other = (x * NC + c + d) % (n_tp * NC)
-        return device(z, y, other % NC, other // NC)
+        other = lax.rem(x * NC + c + d, n_tp * NC)
+        return device(z, y, lax.rem(other, NC), lax.div(other, NC))
+
+    wqk[...] = jnp.zeros_like(wqk)
+    wv[...] = jnp.zeros_like(wv)
+    wot[...] = jnp.zeros_like(wot)
+    wd[...] = jnp.zeros_like(wd)
+
+    barrier = pltpu.get_barrier_semaphore()
+
+    def greet(to):
+        pl.semaphore_signal(barrier, inc=1, device_id=to, device_id_type=MESH)
+
+    each(nyc, lambda d: greet(yc_peer(d)[1]))
+    each(nzc, lambda d: greet(zc_peer(d)[2]))
+    each(n_tp, lambda d: greet(device(z, y, c, lax.rem(x + d, n_tp))))
 
     started = {}
 
@@ -177,11 +195,6 @@
     load("mix_gain", mix_gain_h, mix_gain)
     load("expert_ids", expert_ids_h, expert_ids)
     load("expert_weight", expert_weight_h, expert_weight)
-
-    wqk[...] = jnp.zeros_like(wqk)
-    wv[...] = jnp.zeros_like(wv)
-    wot[...] = jnp.zeros_like(wot)
-    wd[...] = jnp.zeros_like(wd)
     own = pl.ds(pl.multiple_of(yc * rows, rows), rows)
     start = yc * rows
     dense_block = start // lanes
@@ -208,15 +221,6 @@
         for name in names:
             started[name].wait()
 
-    barrier = pltpu.get_barrier_semaphore()
-
-    def greet(to):
-        pl.semaphore_signal(barrier, inc=1, device_id=to, device_id_type=MESH)
-
-    each(nyc, lambda d: greet(yc_peer(d)[1]))
-    each(nzc, lambda d: greet(zc_peer(d)[2]))
-    each(n_tp * NC, lambda d: greet(xc_peer(d)))
-
     loaded("tokens", "mix_gain", "expert_ids", "expert_weight")
     wide = tokens[...].astype(F32)
     inverse = lax.rsqrt(jnp.mean(wide * wide, axis=-1, keepdims=True) + eps)
@@ -240,7 +244,7 @@
     meta_own[0:2, :] = packed.astype(BF)
 
     loaded("w_query", "w_key", "w_value", "w_out", "w_dense")
-    pl.semaphore_wait(barrier, (nyc - 1) + (nzc - 1) + (n_tp * NC - 1))
+    pl.semaphore_wait(barrier, (nyc - 1) + (nzc - 1) + (n_tp - 1))
 
     def pair(index):
         return pl.ds(pl.multiple_of(2 * index, 2), 2)
@@ -258,14 +262,14 @@
         send(meta_own.at[0:2, :], meta.at[y, pair(zc), :], sent.at[3], got.at[3], to)
 
     def half_of(index):
-        return nrmh.at[(index * rows) // lanes, 0:2, :]
+        return nrmh.at[lax.div(index * rows, lanes), 0:2, :]
 
     def send_halves(d):
         other, to = yc_peer(d)
         send(half_of(other), tny.at[pair(yc), :], sent.at[16], got.at[16], to)
 
     def z_peer(d):
-        return device((z + d) % nz, y, c, x)
+        return device(lax.rem(z + d, nz), y, c, x)
 
     mine_p, mine_o = wqk.at[own, :], wot.at[own, :]
     mine_v, mine_d = wv.at[z, dense_rows, :], wd.at[z, dense_rows, :]
@@ -316,7 +320,9 @@
     new_m_value = jnp.zeros(state_m.shape, F32)
     for h in range(head_count):
         new_m_value = jnp.where(m_lane == h, ms[h], new_m_value)
-    new_m[...] = new_m_value
+    m_out[...] = new_m_value
+    store_m = pltpu.make_async_copy(m_out, new_m, loads.at[1])
+    store_m.start()
 
     keep_n.wait()
     wait_for(count.at[0 : nzc - 1, :, 0:block], got.at[1])
@@ -374,7 +380,7 @@
             c_new = decay * c_in[t, h] + inflow * outer
             c_out[t, h] = c_new
             n_new = decay * state_n[t, h : h + 1, :] + inflow * kf[t : t + 1, :]
-            new_n[t, h : h + 1, :] = n_new
+            n_out[t, h : h + 1, :] = n_new
             numer = mm(qf, c_new, precision=lax.Precision.HIGHEST)
             denom = jnp.sum(qf[t : t + 1, :] * n_new, axis=-1, keepdims=True)
             denom = jnp.maximum(jnp.abs(denom), 1.0)
@@ -383,6 +389,8 @@
 
     store_c = pltpu.make_async_copy(c_out, new_c, loads.at[5])
     store_c.start()
+    store_n = pltpu.make_async_copy(n_out, new_n, loads.at[2])
+    store_n.start()
 
     keep_h = pltpu.make_async_copy(hb.at[0:2, :], hg.at[pair(zc), :], loads.at[4])
     keep_h.start()
@@ -429,13 +437,13 @@
 
     def spread(ref, r):
         for d in sorted(range(1, nz), key=lambda d: -min(d, nz - d)):
-            send(ref, ref, sent.at[11], r.at[d], at((sa + d) % nz, sb))
-
-    for d in ring:
-        send(mine, mine, sent.at[10], got_y.at[d], at(sa, (sb + d) % NY))
+            send(ref, ref, sent.at[11], r.at[d], at(lax.rem(sa + d, nz), sb))
+
+    for d in reversed(ring):
+        send(mine, mine, sent.at[10], got_y.at[d], at(sa, lax.rem(sb + d, NY)))
     spread(mine, got_z)
     for index, d in enumerate(ring):
-        block_in = ag.at[c, sa, (sb + NY - d) % NY]
+        block_in = ag.at[c, sa, lax.rem(sb + NY - d, NY)]
         wait_for(block_in, got_y.at[d])
         spread(block_in, got_z if index < near else got_far)
 
@@ -447,7 +455,7 @@
     for d in lines:
         wait_for(ag.at[0, 0, 0 : near + 1], got_z.at[d])
         wait_for(ag.at[0, 0, near + 1 : NY], got_far.at[d])
-        swap(ag.at[c, (sa + nz - d) % nz])
+        swap(ag.at[c, lax.rem(sa + nz - d, nz)])
     wait_for(meta.at[0 : NY - 1], got.at[6])
     loaded("moe_gain", "w_group", "w_dense_gate", "w_gate", "w_up", "w_down")
     side = seqs // 2
@@ -457,6 +465,20 @@
         return jnp.concatenate(pieces, axis=0)
 
     expert = ep.astype(F32)
+
+    local_row = iota((n_ep // 2, side), 1)
+    local_slot = (local_row % half) // (2 * NC) * nyc
+    local_slot = local_slot + (local_row // half) * NC + (local_row % (2 * NC)) // 2
+    placing = ones_where(local_slot == iota((n_ep // 2, side), 0))
+    quarter = nz // 2
+    order = [0] + sorted(range(1, quarter), key=lambda k: -abs(2 * k - quarter))
+
+    def rows_at(h, j):
+        z_ = h * quarter + (z % quarter + j) % quarter
+        return z_, pl.ds(pl.multiple_of(z_ * nyc, nyc), nyc)
+
+    def first_or_second(h):
+        return (h + c) % 2
 
     def run_half(h):
         squares = jnp.zeros((side, block), F32)
@@ -477,7 +499,23 @@
         meta_rows[at_rows, :] = facts
         ids = facts.astype(F32)
         assigned = (ids[:, 0:1] == expert) | (ids[:, 1:2] == expert)
-        hidden[at_rows, :] = jnp.where(assigned, act, 0.0).astype(BF)
+        masked = jnp.where(assigned, act, 0.0).astype(BF)
+        slots = mm(placing, masked).astype(BF)
+        at_slots = pl.ds(pl.multiple_of(h * (n_ep // 2), n_ep // 2), n_ep // 2)
+
+        def down(x_):
+            cut = pl.ds(pl.multiple_of(x_ * share, share), share)
+            return mm(slots, wdn[:, cut]).astype(BF)
+
+        for d in range(1, n_tp):
+            dp[d, at_slots, :] = down((x + d) % n_tp)
+        for j in order:
+            at_block = rows_at(h, j)[1]
+            for d in sorted(range(1, n_tp), key=lambda d: -min(d, n_tp - d)):
+                to = device(z, y, c, (x + d) % n_tp)
+                got_b = got_x.at[first_or_second(h) * (nz // 2) + j]
+                send(dp.at[d, at_block], xg.at[x, at_block], sent.at[13], got_b, to)
+        xg[x, at_slots, :] = down(x)
 
     run_half(c)
     wait_for(ag.at[0], got.at[11])
@@ -488,26 +526,6 @@
         h, y_, rest = r // side, (r // half) % NY, r % half
         z_ = h * (nz // 2) + rest // (2 * NC)
         return ((z_ * NY + y_) * NC) * 2 + rest % (2 * NC)
-
-    slot_rows = iota((n_ep, seqs), 0)
-    placing = ones_where(token_of((n_ep, seqs)) // 2 == slot_rows)
-    slots = mm(placing, hidden[...]).astype(BF)
-
-    def down(x_):
-        return mm(slots, wdn[:, pl.ds(pl.multiple_of(x_ * share, share), share)]).astype(BF)
-
-    for d in range(1, n_tp):
-        dp[d] = down((x + d) % n_tp)
-    order = sorted(range(nz), key=lambda k: -min(k, nz - k))
-
-    def rows_at(k):
-        return pl.ds(pl.multiple_of(((z + k) % nz) * nyc, nyc), nyc)
-
-    for k in order:
-        for d in sorted(range(1, n_tp), key=lambda d: -min(d, n_tp - d)):
-            to = device(z, y, c, (x + d) % n_tp)
-            send(dp.at[d, rows_at(k)], xg.at[x, rows_at(k)], sent.at[13], got_x.at[k], to)
-    xg[x] = down(x)
 
     local = ones_where(token_of((2 * nyc, seqs)) == z * 2 * nyc + iota((2 * nyc, seqs), 0))
     picks = mm(local, meta_rows[...])
@@ -544,6 +562,7 @@
         mixing = mixing + jnp.where(same & (ident == source), route, 0.0)
     mix_hi = mixing.astype(BF)
     mix_lo = (mixing - mix_hi.astype(F32)).astype(BF)
+    mix_both = jnp.concatenate([mix_hi, mix_lo], axis=1)
     owned = ones_where(
         (token_of((16, seqs)) == 2 * ep + iota((16, seqs), 0)) & (iota((16, seqs), 0) < 2)
     )
@@ -556,19 +575,30 @@
             + mm(owned[:, side:], ag[1, :, b].reshape(side, block))
         )
 
-    for k in order:
-        wait_for(xg.at[0 : n_tp - 1, 0:nyc, :], got_x.at[k])
-        total_out = xg[0, rows_at(k), :].astype(F32)
-        for j in range(1, n_tp):
-            total_out = total_out + xg[j, rows_at(k), :].astype(F32)
-        if k == 0:
-            zg[z] = total_out.astype(BF)
-        else:
-            eo[rows_at(k), :] = total_out.astype(BF)
-            send(eo.at[rows_at(k), :], zg.at[z], sent.at[14], got.at[13], z_peer(k))
+    for turn in range(2):
+        for j in order:
+            z_, at_block = rows_at((c + turn) % 2, j)
+            wait_for(xg.at[0 : n_tp - 1, 0:nyc, :], got_x.at[turn * quarter + j])
+            total_out = xg[0, at_block, :].astype(F32)
+            for k in range(1, n_tp):
+                total_out = total_out + xg[k, at_block, :].astype(F32)
+            eo[at_block, :] = total_out.astype(BF)
+
+            def deliver(z_=z_, at_block=at_block):
+                send(eo.at[at_block, :], zg.at[z], sent.at[14], got.at[13], device(z_, y, c, x))
+
+            def keep(at_block=at_block):
+                zg[z] = eo[at_block, :]
+
+            if j == 0:
+                pl.when(z_ != z)(deliver)
+                pl.when(z_ == z)(keep)
+            else:
+                deliver()
     wait_for(zg.at[0 : nz - 1], got.at[13])
     arrived = zg[...].reshape(n_ep, share)
-    ys[...] = (mm(mix_hi, arrived) + mm(mix_lo, arrived) + dense).astype(BF)
+    twice = jnp.concatenate([arrived, arrived], axis=0)
+    ys[...] = (mm(mix_both, twice) + dense).astype(BF)
     keep_y = pltpu.make_async_copy(ys.at[pair(yc), :], yg.at[pair(yc), :], loads.at[4])
     keep_y.start()
 
@@ -582,9 +612,12 @@
     summed = mm(pair_sum(nyc), yg[...])
     for k in range(per_share):
         at_cols = slice(k * block, (k + 1) * block)
-        mixed[:, at_cols] = (residual[k] + summed[:, at_cols])[0:2].astype(BF)
-
-    store_c.wait()
+        mixed_out[:, at_cols] = (residual[k] + summed[:, at_cols])[0:2].astype(BF)
+    store_mixed = pltpu.make_async_copy(mixed_out, mixed, loads.at[6])
+    store_mixed.start()
+
+    for copy in (store_c, store_n, store_m):
+        copy.wait()
     wait_for(wqk.at[0 : (NY - 1) * rows, :], sent.at[0])
     wait_for(count.at[0 : nyc - 1, :, 0 : nz * lanes], sent.at[16])
     wait_for(wv.at[0 : nz - 1, 0:rows, :], sent.at[17])
@@ -604,6 +637,7 @@
     wait_for(xg.at[0 : n_tp - 1], sent.at[13])
     wait_for(zg.at[0 : nz - 1], sent.at[14])
     wait_for(count.at[0 : nyc - 1, :, 0:share], sent.at[15])
+    store_mixed.wait()
 
 
 def per_device(
@@ -639,7 +673,6 @@
     nzc, nyc = nz * NC, NY * NC
     hidden = w_exp_gate.shape[2]
     qkv = 2 * w_query.shape[1] + w_value.shape[1]
-    vm = pl.BlockSpec(memory_space=pltpu.VMEM)
     anywhere = pl.BlockSpec(memory_space=pltpu.HBM)
     V = pltpu.VMEM
 
@@ -671,13 +704,15 @@
         V((2 * nyc, w_value.shape[1]), BF),
         V(state_c.shape, F32),
         V(state_c.shape, F32),
+        V(state_n.shape, F32),
+        V(state_m.shape, F32),
+        V((2, share), BF),
         V((16, w_output.shape[0]), BF),
         V((2 * nzc, w_output.shape[0]), BF),
         V((2 * nzc, block), BF),
         V((n_tp * NC, nzc, block), BF),
         V((2, nz, NY, nzc, block), BF),
         V((2 * n_ep, width), BF),
-        V((2 * n_ep, hidden), BF),
         V((2 * n_ep, 128), BF),
         V((2 * nyc, width), BF),
         V((width, hidden), BF),
@@ -715,7 +750,7 @@
         name="layer",
         out_shape=out_shape,
         in_specs=in_specs,
-        out_specs=(vm, anywhere, vm, vm),
+        out_specs=(anywhere,) * 4,
         scratch_shapes=scratch,
         compiler_params=pltpu.CompilerParams(
             collective_id=0, has_side_effects=True, vmem_limit_bytes=67043328

time: 73.1 us -> 69.6 us (0.952)
  Pallas kernels: 72.3 us -> 68.8 us
    pallas_call x1, Pallas kernels: 70.4 us -> 66.9 us  [per_device(): pl.pallas_call(kernel, name='layer', out_shape=out_shape, in_specs=in_spe...]
where the time goes in v3:
time: 69.6 us; the launch traced here: 69.4 us
  Pallas kernels  68.8 us (99%)
    pallas_call x1, Pallas kernels, per_device(): pl.pallas_call(kernel, name='layer', out_shape=out_shape, in_specs=in_spe...  66.9 us
    pallas_call x1, Pallas kernels, per_device(): pl.pallas_call(store_kernel, name='store', out_shape=out_shape, in_specs=...  1.91 us

profile of v3, /device:TPU:1, one launch (start us, length us, event | category | flops | bytes accessed | tf_op | source)
XLA Modules:
  0.0 69.4 jit_solution(4289112588449884563)
XLA Ops:
  0.6 66.9 %layer.1 = (bf16[2,512]{1,0:T(2,128)(2,1)}, f32[2,2,128,256]{3,2,1,0:T(8,128)}, f32[2,2,128]{2,1,0:T(2,128)}, f32[2,2]{1,0:T(2,128)}) custom-call(bf16[2,2048]{1,0:T(2,128)(2,1)} %refs_0_.1, f32[2,2,128,256]{3,2,1,0:T(8,128)} %refs_1_.1, f32[2,2,128]{2,1,0:T(2,128)} %refs_2_.1, f32[2,2]{1,0:T(2,128)} %refs_3_.1, f32[1,2048]{1,0:T(1,128)} %bitcast.12, ...), custom_call_target="tpu_custom_call" | custom-call | tf_op jit(solution)/shard_map/layer/pallas_call | solution.py:748
  67.5 1.9 %store.1 = (bf16[2,512]{1,0:T(2,128)(2,1)}, f32[2,2,128,256]{3,2,1,0:T(8,128)}, f32[2,2,128]{2,1,0:T(2,128)}, f32[2,2]{1,0:T(2,128)}) custom-call(bf16[2,512]{1,0:T(2,128)(2,1)} %get-tuple-element.8.refs_0_, f32[2,2,128,256]{3,2,1,0:T(8,128)} %get-tuple-element.9.refs_1_, f32[2,2,128]{2,1,0:T(2,128)} %get-tuple-element.10.refs_2_, ...), custom_call_target="tpu_custom_call" | custom-call | tf_op jit(solution)/shard_map/store/pallas_call | solution.py:781
